TPU v7x, 128 devices: a whole 4x4x4 slice. The times are simulated.
128 devices in a mesh: ep: 16 (over z, x), tp: 8 (over y, core).
Axes of the slice: x: 4, y: 4, z: 4, core: 2. Of those that a mesh axis runs over, the one named last changes fastest.
Arguments:
- mixer_rows: bfloat16 [4096, 4096], P('ep'), may hold values from -8 to 8, as said below
- mixer_gain: float32 [4096], replicated, may hold values from 0.1 to 1.9
- gate_proj: bfloat16 [4096, 4096], P(None, 'tp'), may hold values from -0.09375 to 0.09375
- input_proj: bfloat16 [4096, 4096], P(None, 'tp'), may hold values from -0.09375 to 0.09375
- conv_taps: float32 [4, 4096], P(None, 'tp'), may hold values from -2 to 2
- input_gates: bfloat16 [16, 256, 256], P('tp'), may hold values from -0.375 to 0.375
- decay_gates: bfloat16 [16, 256, 256], P('tp'), may hold values from -0.375 to 0.375
- decay_offset: float32 [4096], P('tp'), may hold values from 4.8 to 13, as said below
- out_proj: bfloat16 [4096, 4096], P('tp'), may hold values from -0.09375 to 0.09375
- mixer_scale: float32 [4096], replicated, may hold values from 0.1 to 1.9
- expert_rows: bfloat16 [4096, 4096], P('ep'), may hold values from -6 to 6
- expert_gain: float32 [4096], replicated, may hold values from 0.1 to 1.9
- route_ids: int32 [4096, 2], P('ep'), may hold values from 0 to 15, all different within a row; in each aligned block of 256 rows (0 to 255, 256 to 511, ...) at most 48 rows name the same one
- route_weights: float32 [4096, 2], P('ep'), may hold values from 0.5 to 2
- expert_gate: bfloat16 [16, 4096, 1024], P('ep', None, 'tp'), may hold values from -0.09375 to 0.09375
- expert_up: bfloat16 [16, 4096, 1024], P('ep', None, 'tp'), may hold values from -0.09375 to 0.09375
- expert_down: bfloat16 [16, 1024, 4096], P('ep', 'tp'), may hold values from -0.1875 to 0.1875
- shared_gate: bfloat16 [4096, 1024], P(None, 'tp'), may hold values from -0.09375 to 0.09375
- shared_up: bfloat16 [4096, 1024], P(None, 'tp'), may hold values from -0.09375 to 0.09375
- shared_down: bfloat16 [1024, 4096], P('tp'), may hold values from -0.1875 to 0.1875
- expert_scale: float32 [4096], replicated, may hold values from 0.1 to 1.9
Outputs:
- mixer_out: bfloat16 [4096, 4096], P(('ep', 'tp'))
- expert_out: bfloat16 [4096, 4096], P(('ep', 'tp'))
Inputs may be any that keep to these rules, and one draw needn't show every extreme that they name: `mixer_rows`: order one, with a common direction whose weight drifts slowly along the sequence. `decay_offset`: the even channels forget within some 30 to 200 tokens; the odd channels keep 5 to 90 percent of their state over the whole sequence of 4096 tokens. `route_ids`: each row names 2 different experts; within the rows of one index of ep (aligned blocks of 256 rows) no expert is named by more than 48 rows, and in some blocks one is named by exactly 48.
All inputs are finite; a program needn't handle non-finite values.
Results may differ from a plain program's by a relative error of at most 0.0033.
The roundings to bfloat16 on the way count: a program that leaves them out, or rounds other values in their place, can miss the bound.
Values may be sent and summed in bfloat16 or wider, within the bound.
A program may use at most 192 MiB of HBM per device.

v0:
```python
import jax
import jax.numpy as jnp
from jax import lax
from jax.sharding import PartitionSpec as P

eps = 1e-06
lru_power = 8.0


def shifted(block, axis, distance):
    devices = range(lax.axis_size(axis))
    route = [(i - distance, i) for i in devices if i - distance in devices]
    return lax.ppermute(block, axis, route)


def sent_to_all(shard, axis):
    length = lax.axis_size(axis)
    return lax.all_to_all(
        jnp.broadcast_to(shard[None], (length, *shard.shape)), axis, 0, 0, tiled=True
    )


def collected_together(shard, axis):
    leaves = jax.tree.leaves(shard)
    turns = sorted(range(len(leaves)), key=lambda k: -leaves[k].size)
    width = (1, *leaves[turns[0]].shape)[-1]
    lines = [
        jnp.pad(leaves[k].reshape(-1), (0, -leaves[k].size % width)).reshape(-1, width)
        for k in turns
    ]
    both, at, found = (sent_to_all(jnp.concatenate(lines), axis), 0, {})
    for k, line in zip(turns, lines):
        share = both[:, at : at + len(line)].reshape(len(both), -1)
        found[k] = share[:, : leaves[k].size].reshape(-1, *leaves[k].shape)
        at += len(line)
    numbers = iter(range(len(leaves)))
    return jax.tree.map(lambda _: found[next(numbers)], shard)


def folded_in_pairs(pieces, combine):
    while len(jax.tree.leaves(pieces)[0]) > 1:
        pieces = jax.vmap(combine)(
            *(jax.tree.map(lambda part: part[side::2], pieces) for side in (0, 1))
        )
    return jax.tree.map(lambda part: part[0], pieces)


def carried_in(shard, axis, combine, identity):
    length, mine = (lax.axis_size(axis), lax.axis_index(axis))
    passed = jnp.arange(length) < mine

    def kept(part, zero, own):
        part = jnp.where(
            passed.reshape(-1, *(1 for _ in own.shape)), part, jnp.asarray(zero, own.dtype)
        )
        return part

    pieces = collected_together(shard, axis)
    return folded_in_pairs(jax.tree.map(kept, pieces, identity, shard), combine)


def sent_together(arrays, axis, dim, along):
    both = jnp.concatenate(arrays, axis=along)
    whole, at, outs = (lax.psum_scatter(both, axis, scatter_dimension=dim, tiled=True), 0, [])
    for a in arrays:
        outs.append(lax.slice_in_dim(whole, at, at + a.shape[along], axis=along))
        at += a.shape[along]
    return tuple(outs)


def rms_scale(values, scale):
    floats = values.astype(jnp.float32)
    return floats * lax.rsqrt(jnp.mean(floats * floats, axis=-1, keepdims=True) + eps) * scale


def linear_pair(earlier, later):
    return (earlier[0] * later[0], later[0] * earlier[1] + later[1])


def slot_table(route_ids, expert_count, capacity):
    id_list = route_ids.reshape(-1)
    indicator = (id_list[:, None] == jnp.arange(expert_count, dtype=jnp.int32)[None, :]).astype(
        jnp.int32
    )
    earlier_count = jnp.cumsum(indicator, axis=0) - indicator
    position = jnp.sum(earlier_count * indicator, axis=1)
    slot_ids = id_list * capacity + position
    matched = (
        slot_ids[None, :] == jnp.arange(expert_count * capacity, dtype=jnp.int32)[:, None]
    ).astype(jnp.int32)
    source = jnp.sum(matched * jnp.arange(id_list.shape[0], dtype=jnp.int32)[None, :], axis=1)
    filled = jnp.sum(matched, axis=1) > 0
    return (slot_ids, source, filled)


def body(
    mixer_rows,
    mixer_gain,
    gate_proj,
    input_proj,
    conv_taps,
    input_gates,
    decay_gates,
    decay_offset,
    out_proj,
    mixer_scale,
    expert_rows,
    expert_gain,
    route_ids,
    route_weights,
    expert_gate,
    expert_up,
    expert_down,
    shared_gate,
    shared_up,
    shared_down,
    expert_scale,
):
    row_count = mixer_rows.shape[0]
    normed = rms_scale(mixer_rows, mixer_gain).astype(jnp.bfloat16)
    gate_branch = jax.nn.gelu(jnp.dot(normed, gate_proj, preferred_element_type=jnp.float32))
    branch = jnp.dot(normed, input_proj, preferred_element_type=jnp.float32).astype(jnp.bfloat16)
    tap_count = conv_taps.shape[0]
    earlier_rows = shifted(branch[row_count - tap_count + 1 :], "ep", 1)
    padded = jnp.concatenate([earlier_rows, branch], axis=0)
    conv_sum = conv_taps[0] * padded[0:row_count].astype(jnp.float32)
    for tap_index in range(1, tap_count):
        conv_sum = conv_sum + conv_taps[tap_index] * padded[
            tap_index : tap_index + row_count
        ].astype(jnp.float32)
    conv_out = conv_sum.astype(jnp.bfloat16)
    block_rows = conv_out.reshape(row_count, input_gates.shape[0], input_gates.shape[1])
    input_gate = jax.nn.sigmoid(
        jnp.einsum("rbi,bij->rbj", block_rows, input_gates, preferred_element_type=jnp.float32)
    ).reshape(row_count, -1)
    decay_gate = jax.nn.sigmoid(
        jnp.einsum("rbi,bij->rbj", block_rows, decay_gates, preferred_element_type=jnp.float32)
    ).reshape(row_count, -1)
    log_decay = -lru_power * decay_gate * jax.nn.softplus(-decay_offset)
    positions = lax.axis_index("ep") * row_count + jnp.arange(row_count, dtype=jnp.int32)
    input_scale = jnp.where((positions == 0)[:, None], 1.0, jnp.sqrt(-jnp.expm1(2.0 * log_decay)))
    drive_term = input_scale * input_gate * conv_out.astype(jnp.float32)
    decay_rate = jnp.exp(log_decay)
    decay_product, local_states = lax.associative_scan(
        linear_pair, (decay_rate, drive_term), axis=0
    )
    carried = carried_in(
        (decay_product[-1], local_states[-1]),
        "ep",
        linear_pair,
        (jnp.ones_like(decay_rate[0]), jnp.zeros_like(decay_rate[0])),
    )
    states = local_states + decay_product * carried[1][None, :]
    gated_rows = (gate_branch * states).astype(jnp.bfloat16)
    mixer_term = jnp.dot(gated_rows, out_proj, preferred_element_type=jnp.float32)
    ep_size = lax.axis_size("ep")
    local_experts = expert_gate.shape[0]
    expert_count = local_experts * ep_size
    top_count = route_ids.shape[1]
    token_count = expert_rows.shape[0]
    row_width = expert_rows.shape[1]
    capacity = token_count * top_count * 3 // (2 * expert_count)
    expert_normed = rms_scale(expert_rows, expert_gain).astype(jnp.bfloat16)
    slot_ids, source, filled = slot_table(route_ids, expert_count, capacity)
    outgoing = jnp.where(
        filled[:, None], expert_normed[source // top_count], jnp.zeros((), jnp.bfloat16)
    )
    outgoing = outgoing.reshape(ep_size, local_experts, capacity, row_width)
    received = lax.all_to_all(outgoing, "ep", split_axis=0, concat_axis=0, tiled=True)
    gate_part = jnp.einsum(
        "secd,edf->secf", received, expert_gate, preferred_element_type=jnp.float32
    )
    up_part = jnp.einsum("secd,edf->secf", received, expert_up, preferred_element_type=jnp.float32)
    copy_hidden = (jax.nn.silu(gate_part) * up_part).astype(jnp.bfloat16)
    column_sums = lax.psum_scatter(
        jnp.einsum("secf,efd->secd", copy_hidden, expert_down, preferred_element_type=jnp.float32),
        "tp",
        scatter_dimension=3,
        tiled=True,
    )
    result = lax.all_to_all(column_sums, "ep", split_axis=0, concat_axis=0, tiled=True)
    flat_back = result.reshape(expert_count * capacity, -1)
    picked = flat_back[slot_ids] * route_weights.reshape(-1, 1)
    routed = jnp.sum(picked.reshape(token_count, top_count, -1), axis=1)
    shared_hidden = (
        jax.nn.silu(jnp.dot(expert_normed, shared_gate, preferred_element_type=jnp.float32))
        * jnp.dot(expert_normed, shared_up, preferred_element_type=jnp.float32)
    ).astype(jnp.bfloat16)
    shared_term = jnp.dot(shared_hidden, shared_down, preferred_element_type=jnp.float32)
    mixer_sum, expert_sum = sent_together((mixer_term, shared_term), "tp", 0, 1)
    expert_sum = expert_sum + lax.all_to_all(routed, "tp", split_axis=0, concat_axis=1, tiled=True)
    mixer_out = rms_scale(mixer_sum, mixer_scale).astype(jnp.bfloat16)
    expert_out = rms_scale(expert_sum, expert_scale).astype(jnp.bfloat16)
    return (mixer_out, expert_out)


def solution(mesh):
    placed = (
        P("ep", None),
        P(),
        P(None, "tp"),
        P(None, "tp"),
        P(None, "tp"),
        P("tp", None, None),
        P("tp", None, None),
        P("tp"),
        P("tp", None),
        P(),
        P("ep", None),
        P(),
        P("ep", None),
        P("ep", None),
        P("ep", None, "tp"),
        P("ep", None, "tp"),
        P("ep", "tp", None),
        P(None, "tp"),
        P(None, "tp"),
        P("tp", None),
        P(),
    )
    return jax.shard_map(
        body,
        mesh=mesh,
        in_specs=placed,
        out_specs=(P(("ep", "tp"), None), P(("ep", "tp"), None)),
        check_vma=False,
    )
```

profile of v0, /device:TPU:1, one launch (start us, length us, event | category | flops | bytes accessed | tf_op | source)
XLA Modules:
  0.0 264.7 jit_solution(15755040382263902929)
XLA Ops:
  7.2 0.9 copy.64
  8.1 0.1 eq.51
  8.3 0.1 reshape.247
  8.4 2.1 fusion.7
  10.5 1.2 reduce-window.6
  11.7 0.2 slice_reduce_fusion
  12.0 0.5 convert_reduce_fusion
  12.7 2.2 fusion.9
  14.9 5.7 %gather_fusion = bf16[768,4096]{1,0:T(8,128)(2,1)} fusion(bf16[256,4096]{1,0:T(8,128)(2,1)S(1)} %fusion.9, s32[1024]{0:T(1024)S(1)} %pad_clamp_fusion.1), kind=kCustom, calls=%fused_computation | custom fusion | bytes 12585984 | tf_op jit(solution)/shard_map/gather | solution.py:166
  20.6 3.3 %broadcast_select_fusion = bf16[16,1,48,4096]{3,2,1,0:T(8,128)(2,1)S(1)} fusion(bf16[16,1,48,4096]{3,2,1,0:T(8,128)(2,1)} %bitcast.125, pred[16,48]{1,0:T(8,128)(4,1)S(1)} %gt.11), kind=kLoop, calls=%fused_computation.8 | loop fusion | flops 3145728 | bytes 12583680 | tf_op jit(solution)/shard_map/jit(_where)/select_n | solution.py:165
  23.9 80.6 %all_to_all.34 = bf16[16,1,48,4096]{3,2,1,0:T(8,128)(2,1)S(1)} all-to-all(bf16[16,1,48,4096]{3,2,1,0:T(8,128)(2,1)S(1)} %broadcast_select_fusion), channel_id=1, replica_groups=mesh['ep'=16,'tp'=8] {'ep'}, dimensions={0} | all-to-all | bytes 12582912 | tf_op jit(solution)/shard_map/all_to_all | solution.py:169
  104.5 2.6 copy-done.2
  107.1 1.8 fusion.16
  108.9 14.1 %convolution_bitcast_fusion = f32[16,1,48,4096]{3,2,0,1:T(8,128)} fusion(bf16[1,128,4096]{2,1,0:T(8,128)(2,1)S(1)} %copy-done, bf16[16,1,48,4096]{3,2,1,0:T(8,128)(2,1)} %copy-done.2, bf16[1,4096,128]{2,1,0:T(8,128)(2,1)} %param.36, f32[16,1,48,128]{3,2,0,1:T(8,128)S(1)} %fusion.16), kind=kOutput, calls=%fused_computation.3 | convolution fusion | flops 1611202560 | bytes 21364736 | tf_op jit(solution)/shard_map/secf,efd->secd/dot_general | solution.py:176
  123.1 2.1 fusion.4
  125.2 4.2 %convolution_convert_fusion = bf16[256,512]{1,0:T(8,128)(2,1)S(1)} fusion(bf16[4096,512]{1,0:T(8,128)(2,1)} %param.24, bf16[256,4096]{1,0:T(8,128)(2,1)} %param.21, f32[4096]{0:T(1024)S(1)} %copy-done.8, f32[256]{0:T(256)S(1)} %add_rsqrt_fusion.1), kind=kOutput, calls=%fused_computation.32 | convolution fusion | flops 1078067200 | bytes 6571008 | tf_op jit(solution)/shard_map/dot_general | solution.py:122
  129.4 0.6 slice.435
  130.0 2.8 %collective-permute-start = (bf16[3,512]{1,0:T(4,128)(2,1)}, bf16[3,512]{1,0:T(4,128)(2,1)}, u32[]{:S(2)}, u32[]{:S(2)}) collective-permute-start(bf16[3,512]{1,0:T(4,128)(2,1)} %slice.435), channel_id=1, source_target_pairs={{0,8},{8,16},{16,24},{24,32},{32,40},{40,48},{48,56},{56,64},{64,7... | collective-permute-start | bytes 9224 | tf_op jit(solution)/shard_map/ppermute | solution.py:13
  132.8 0.6 fusion.104
  133.4 0.6 fusion.115
  134.0 0.7 fusion.117
  134.7 4.9 %fusion.32 = f32[256,4096]{1,0:T(8,128)} fusion(bf16[128,4096]{1,0:T(8,128)(2,1)} %param.40, bf16[256,4096]{1,0:T(8,128)(2,1)S(1)} %fusion.9, bf16[4096,128]{1,0:T(8,128)(2,1)} %param.39, f32[256,128]{1,0:T(8,128)S(1)} %fusion.117), kind=kOutput, calls=%fused_computation.38 | convolution fusion | flops 537067520 | bytes 8519680 | tf_op jit(solution)/shard_map/dot_general | solution.py:189
  139.7 1.0 add_convert_fusion
  140.7 0.4 fusion.13
  141.1 0.2 copy.74
  141.3 0.4 fusion.15
  141.6 0.2 copy.75
  141.8 0.4 convert_multiply_fusion.4
  142.3 0.3 slice.337
  142.6 0.3 slice.338
  142.9 0.3 slice.336
  143.3 0.3 slice.340
  143.7 0.1 slice.343
  145.0 0.2 slice.341
  145.2 0.2 slice.390
  145.4 1.4 slice.335
  146.8 1.4 slice.392
  149.4 1.7 pad.129
  151.3 2.0 fusion.74
  153.3 0.7 pad_maximum_fusion.3
  154.0 1.1 pad.128
  155.1 1.7 pad.113
  156.8 1.0 pad_maximum_fusion.2
  157.8 1.8 pad.112
  159.5 0.7 slice_add_fusion.3
  160.3 0.7 slice_add_fusion.2
  161.0 0.6 broadcast_in_dim.44
  161.7 4.9 %all-to-all-start = ((f32[16,2,512]{2,1,0:T(2,128)}), f32[16,2,512]{2,1,0:T(2,128)S(1)}, u32[]{:S(2)}, u32[]{:S(2)}) async-start(f32[16,2,512]{2,1,0:T(2,128)} %broadcast_in_dim.44), calls=%async_computation | async-start | bytes 131072 | tf_op jit(solution)/shard_map/all_to_all | solution.py:18
  166.6 6.5 %all-to-all-done = f32[16,2,512]{2,1,0:T(2,128)S(1)} async-done(((f32[16,2,512]{2,1,0:T(2,128)}), f32[16,2,512]{2,1,0:T(2,128)S(1)}, u32[]{:S(2)}, u32[]{:S(2)}) %all-to-all-start) | async-done | bytes 65568 | tf_op jit(solution)/shard_map/all_to_all | solution.py:18
  173.5 8.6 %fusion.59 = f32[256,4096]{1,0:T(8,128)} fusion(bf16[512,4096]{1,0:T(8,128)(2,1)} %param.29, bf16[4096,512]{1,0:T(8,128)(2,1)} %param.23, bf16[256,4096]{1,0:T(8,128)(2,1)S(1)} %copy-done.3, f32[4096]{0:T(1024)S(1)} %copy-done.9, f32[256]{0:T(256)S(1)} %copy-done.15, f32[256,512]{1,0:T(8,128)S(1)} %pad.128, f32[256,512]{1,0:T(8,128)S(1)} %copy-done.4, ...), kind=kOutput, calls=%fused_computation.54 | convolution fusion | flops 2153512960 | bytes 16796672 | tf_op jit(solution)/shard_map/dot_general | solution.py:155
  182.1 7.7 %pad_maximum_fusion = f32[256,8192]{1,0:T(8,128)} fusion(f32[256,4096]{1,0:T(8,128)} %fusion.32, f32[256,4096]{1,0:T(8,128)} %fusion.59), kind=kLoop, calls=%fused_computation.2 | loop fusion | flops 2097152 | bytes 16777216 | tf_op jit(solution)/shard_map/concatenate | solution.py:63
  189.9 4.3 %reduce-scatter.5.cloned.1.call-done = f32[16,1,48,512]{3,2,0,1:T(8,128)} async-done(((f32[16,1,48,4096]{3,2,0,1:T(8,128)}), f32[16,1,48,512]{3,2,0,1:T(8,128)}) %reduce-scatter.5.cloned.1.call-update) | async-done | bytes 1572880 | tf_op jit(solution)/shard_map/reduce_scatter | solution.py:175
  194.1 6.7 %all-to-all-start.2 = ((f32[16,1,48,512]{3,2,1,0:T(8,128)}), f32[16,1,48,512]{3,2,1,0:T(8,128)S(1)}, u32[]{:S(2)}, u32[]{:S(2)}) async-start(f32[16,1,48,512]{3,2,1,0:T(8,128)} %bitcast.130), calls=%async_computation.4 | async-start | bytes 3145728 | tf_op jit(solution)/shard_map/all_to_all | solution.py:181
  200.8 0.1 copy.69
  201.0 0.1 mul.443
  201.1 0.1 copy.70
  201.3 20.8 %all-to-all-done.2 = f32[16,1,48,512]{3,2,1,0:T(8,128)S(1)} async-done(((f32[16,1,48,512]{3,2,1,0:T(8,128)}), f32[16,1,48,512]{3,2,1,0:T(8,128)S(1)}, u32[]{:S(2)}, u32[]{:S(2)}) %all-to-all-start.2) | async-done | bytes 1572896 | tf_op jit(solution)/shard_map/all_to_all | solution.py:181
  222.1 2.3 gather_fusion.1
  224.4 2.0 gather.13
  226.4 1.3 multiply_reduce_fusion
  227.7 22.3 %all_to_all.35 = f32[8,32,512]{2,1,0:T(8,128)S(1)} all-to-all(f32[8,32,512]{2,1,0:T(8,128)S(1)} %bitcast.128), channel_id=1, replica_groups=mesh['ep'=16,'tp'=8] {'tp'}, dimensions={0} | all-to-all | bytes 1048576 | tf_op jit(solution)/shard_map/all_to_all | solution.py:191
  250.1 4.2 %reduce-scatter.3.cloned.1.call-done = f32[32,8192]{1,0:T(8,128)} async-done(((f32[256,8192]{1,0:T(8,128)}), f32[32,8192]{1,0:T(8,128)}) %reduce-scatter.3.cloned.1.call-update) | async-done | bytes 1048592 | tf_op jit(solution)/shard_map/reduce_scatter | solution.py:64
  254.3 1.4 multiply_reduce_fusion.1
  255.7 2.2 multiply_convert_fusion
  (189 shorter events, 3.1 us)
Async XLA Ops:
  7.2 101.7 %copy-start = (bf16[1,128,4096]{2,1,0:T(8,128)(2,1)S(1)}, bf16[1,128,4096]{2,1,0:T(8,128)(2,1)}, u32[]{:S(2)}) copy-start(bf16[1,128,4096]{2,1,0:T(8,128)(2,1)} %param.37) | copy-start | bytes 3145732
  7.2 187.0 %reduce-scatter.5.cloned.1.call-start = ((), (), s32[]{:S(2)}) async-start(), calls=%async_computation.7 | async-start | bytes 14155776 | tf_op jit(solution)/shard_map/reduce_scatter | solution.py:175
  23.9 83.2 %copy-start.18 = (bf16[1,4096,128]{2,1,0:T(8,128)(2,1)S(1)}, bf16[1,4096,128]{2,1,0:T(8,128)(2,1)}, u32[]{:S(2)}) copy-start(bf16[1,4096,128]{2,1,0:T(8,128)(2,1)} %param.35) | copy-start | bytes 3145732
  104.5 2.6 copy-start.2
  123.0 2.1 copy-start.8
  125.2 4.3 %copy-start.14 = (f32[256]{0:T(256)}, f32[256]{0:T(256)S(1)}, u32[]{:S(2)}) copy-start(f32[256]{0:T(256)S(1)} %add_rsqrt_fusion.1) | copy-start | bytes 3076
  125.2 7.6 %copy-start.17 = (f32[512]{0:T(512)S(1)}, f32[512]{0:T(512)}, u32[]{:S(2)}) copy-start(f32[512]{0:T(512)} %param.28) | copy-start | bytes 6148
  125.2 8.2 %copy-start.12 = (f32[4,512]{1,0:T(4,128)S(1)}, f32[4,512]{1,0:T(4,128)}, u32[]{:S(2)}) copy-start(f32[4,512]{1,0:T(4,128)} %param.25) | copy-start | bytes 24580
  125.2 8.8 %copy-start.5 = (bf16[4096,128]{1,0:T(8,128)(2,1)S(1)}, bf16[4096,128]{1,0:T(8,128)(2,1)}, u32[]{:S(2)}) copy-start(bf16[4096,128]{1,0:T(8,128)(2,1)} %param.38) | copy-start | bytes 3145732
  130.0 9.6 %collective-permute-start = (bf16[3,512]{1,0:T(4,128)(2,1)}, bf16[3,512]{1,0:T(4,128)(2,1)}, u32[]{:S(2)}, u32[]{:S(2)}) collective-permute-start(bf16[3,512]{1,0:T(4,128)(2,1)} %slice.435), channel_id=1, source_target_pairs={{0,8},{8,16},{16,24},{24,32},{32,40},{40,48},{48,56},{56,64},{64,7... | collective-permute-start | bytes 9224 | tf_op jit(solution)/shard_map/ppermute | solution.py:13
  134.7 4.9 %copy-start.11 = (f32[1,512]{1,0:T(1,128)S(1)}, f32[1,512]{1,0:T(1,128)}, u32[]{:S(2)}) copy-start(f32[1,512]{1,0:T(1,128)} %get-tuple-element.47) | copy-start | bytes 6148
  134.7 6.0 %copy-start.19 = (bf16[2,256,256]{2,1,0:T(8,128)(2,1)S(1)}, bf16[2,256,256]{2,1,0:T(8,128)(2,1)}, u32[]{:S(2)}) copy-start(bf16[2,256,256]{2,1,0:T(8,128)(2,1)} %param.27) | copy-start | bytes 786436
  139.6 1.6 copy-start.20
  139.6 2.2 copy-start.13
  151.1 22.4 %copy-start.3 = (bf16[256,4096]{1,0:T(8,128)(2,1)S(1)}, bf16[256,4096]{1,0:T(8,128)(2,1)}, u32[]{:S(2)}) copy-start(bf16[256,4096]{1,0:T(8,128)(2,1)} %param.21) | copy-start | bytes 6291460
  151.1 22.4 %copy-start.9 = (f32[4096]{0:T(1024)S(1)}, f32[4096]{0:T(1024)}, u32[]{:S(2)}) copy-start(f32[4096]{0:T(1024)} %param.22) | copy-start | bytes 49156
  151.1 22.4 %copy-start.15 = (f32[256]{0:T(256)S(1)}, f32[256]{0:T(256)}, u32[]{:S(2)}) copy-start(f32[256]{0:T(256)} %copy-done.14) | copy-start | bytes 3076
  153.3 20.2 %copy-start.4 = (f32[256,512]{1,0:T(8,128)S(1)}, f32[256,512]{1,0:T(8,128)}, u32[]{:S(2)}) copy-start(f32[256,512]{1,0:T(8,128)} %pad.129) | copy-start | bytes 1572868
  161.7 11.4 %all-to-all-start = ((f32[16,2,512]{2,1,0:T(2,128)}), f32[16,2,512]{2,1,0:T(2,128)S(1)}, u32[]{:S(2)}, u32[]{:S(2)}) async-start(f32[16,2,512]{2,1,0:T(2,128)} %broadcast_in_dim.44), calls=%async_computation | async-start | bytes 131072 | tf_op jit(solution)/shard_map/all_to_all | solution.py:18
  166.5 87.7 %reduce-scatter.3.cloned.1.call-start = ((), (), s32[]{:S(2)}) async-start(), calls=%async_computation.6 | async-start | bytes 9437184 | tf_op jit(solution)/shard_map/reduce_scatter | solution.py:64
  189.8 11.0 %copy-start.10 = (s32[256,2]{0,1:T(2,128)S(1)}, s32[256,2]{0,1:T(2,128)}, u32[]{:S(2)}) copy-start(s32[256,2]{0,1:T(2,128)} %param.33) | copy-start | bytes 6148
  189.8 11.3 %copy-start.16 = (f32[256,2]{0,1:T(2,128)S(1)}, f32[256,2]{0,1:T(2,128)}, u32[]{:S(2)}) copy-start(f32[256,2]{0,1:T(2,128)} %param.34) | copy-start | bytes 6148
  194.1 27.9 %all-to-all-start.2 = ((f32[16,1,48,512]{3,2,1,0:T(8,128)}), f32[16,1,48,512]{3,2,1,0:T(8,128)S(1)}, u32[]{:S(2)}, u32[]{:S(2)}) async-start(f32[16,1,48,512]{3,2,1,0:T(8,128)} %bitcast.130), calls=%async_computation.4 | async-start | bytes 3145728 | tf_op jit(solution)/shard_map/all_to_all | solution.py:181
  224.4 31.3 %copy-start.6 = (f32[4096]{0:T(1024)S(1)}, f32[4096]{0:T(1024)}, u32[]{:S(2)}) copy-start(f32[4096]{0:T(1024)} %param.41) | copy-start | bytes 49156
  224.4 31.3 %copy-start.7 = (f32[4096]{0:T(1024)S(1)}, f32[4096]{0:T(1024)}, u32[]{:S(2)}) copy-start(f32[4096]{0:T(1024)} %param.30) | copy-start | bytes 49156
  224.4 33.5 %copy-start.1 = (bf16[1,128,4096]{2,1,0:T(8,128)(2,1)S(1)}, bf16[1,128,4096]{2,1,0:T(8,128)(2,1)}, u32[]{:S(2)}) copy-start(bf16[1,128,4096]{2,1,0:T(8,128)(2,1)} %param.37) | copy-start | bytes 3145732
Sparse Core Ops, SparseCore 0:
  123.2 70.9 reduce-scatter.4
  196.5 57.6 reduce-scatter.2
where the time goes:
time: 265 us
  blocking collectives  103 us (39%)
  waiting for transfers between devices  35.7 us (13%)
  matrix products  35 us (13%)
  other arithmetic  32.2 us (12%)
  local copies, waits for them, and re-layouts  29.4 us (11%)
  between operations  15.1 us (6%)
  starting transfers between devices  14.4 us (5%)
    all_to_all x1, blocking collectives, body(): lax.all_to_all(outgoing, 'ep', split_axis=0, concat_axis=0, tiled=True)  80.6 us
    all_to_all x1, blocking collectives, body(): lax.all_to_all(routed, 'tp', split_axis=0, concat_axis=1, tiled=True)  22.3 us
    all_to_all x1, waiting for transfers between devices, body(): lax.all_to_all(column_sums, 'ep', split_axis=0, concat_axis=0, tiled=True)  20.8 us
    dot_general x1, matrix products, body(): jnp.einsum('secf,efd->secd', copy_hidden, expert_down, preferred_element_...  14.1 us
    dot_general x1, matrix products, body(): jnp.dot(gated_rows, out_proj, preferred_element_type=jnp.float32)  8.58 us
    concatenate x1, other arithmetic, sent_together(): both = jnp.concatenate(arrays, axis=along)  7.72 us
    all_to_all x1, starting transfers between devices, body(): lax.all_to_all(column_sums, 'ep', split_axis=0, concat_axis=0, tiled=True)  6.68 us
    pad x28, local copies, waits for them, and re-layouts, body(): lax.associative_scan(linear_pair, (decay_rate, drive_term), axis=0)  6.67 us
  transfers between devices with their start and end apart: 5, of which 4 were waited for; matrix products, arithmetic and copies ran while one was open for 22% of the time, Pallas kernels for 0%

commit v1 on v0

v1 whole, which is shorter than its diff:
```python
import jax
import jax.numpy as jnp
from jax import lax
from jax.experimental import pallas as pl
from jax.experimental.pallas import tpu as pltpu
from jax.sharding import PartitionSpec as P

eps = 1e-06
lru_power = 8.0


def shifted(block, axis, distance):
    devices = range(lax.axis_size(axis))
    route = [(i - distance, i) for i in devices if i - distance in devices]
    return lax.ppermute(block, axis, route)


def rms_scale(values, scale):
    floats = values.astype(jnp.float32)
    return floats * lax.rsqrt(jnp.mean(floats * floats, axis=-1, keepdims=True) + eps) * scale


def linear_pair(earlier, later):
    return (earlier[0] * later[0], later[0] * earlier[1] + later[1])


def slots_of(route_ids, expert_count, capacity):
    named = [
        (route_ids[:, k : k + 1] == jnp.arange(expert_count, dtype=jnp.int32)[None, :])
        for k in range(2)
    ]
    either = jnp.logical_or(*named).astype(jnp.bfloat16)
    count = route_ids.shape[0]
    before = jnp.tril(jnp.ones((count, count), jnp.bfloat16), -1)
    place = jnp.dot(before, either, preferred_element_type=jnp.float32)
    return [
        route_ids[:, k : k + 1] * capacity
        + jnp.sum(jnp.where(named[k], place, 0.0), axis=1, keepdims=True).astype(jnp.int32)
        for k in range(2)
    ]


MESH = pl.DeviceIdType.MESH
NCH = 2
CW = 2048 // NCH


def remote(src, dst, send, recv, device):
    return pltpu.make_async_remote_copy(
        src_ref=src, dst_ref=dst, send_sem=send, recv_sem=recv, device_id=device, device_id_type=MESH
    )


def exchange_kernel(
    send_x, eg, eu, ed, sd, op, sh, acum, loc, gate, cm, whi, wlo, mscale, escale,
    out_m, out_e,
    rows, w_in, w_dn, s_dn, o_pr, sh2, gts, carries, acc, hid, res, back,
    m_part, m_recv, m_sum, m_other, e_part, e_recv, e_sum, e_other,
    d_s, d_r, f_s, f_r, c_s, c_r, p_s, p_r, l_s, r_s, r_r, ms_s, ms_r, es_s, es_r, x_s, x_r,
):
    p = lax.axis_index("ep")
    t = lax.axis_index("tp")
    y = t // 2
    c = t % 2
    o = 1 - c
    par = p % 2
    half = p // 2
    partner = (p, 2 * y + o)

    barrier = pltpu.get_barrier_semaphore()

    def greet(k, _):
        other = (p * 2 + c + k) % 32
        pl.semaphore_signal(
            barrier, inc=1, device_id=(other // 2, 2 * y + other % 2), device_id_type=MESH
        )
        return 0

    lax.fori_loop(1, 32, greet, 0)
    for k in range(1, 4):
        pl.semaphore_signal(
            barrier, inc=1, device_id=(p, 2 * ((y + k) % 4) + c), device_id_type=MESH
        )
    pl.semaphore_wait(barrier, 34)

    def dispatch(step, j):
        i = (half + step) % 8
        return remote(
            send_x.at[i, j], rows.at[(y + 2 * j) % 4, half], d_s.at[i, j], d_r.at[half, j],
            (2 * i + c, 2 * y + 1 - par),
        )

    def arrival(step, j):
        i = (half + 8 - step) % 8
        return i, remote(
            send_x.at[i, j], rows.at[(y + 2 * j) % 4, i], d_s.at[i, j], d_r.at[i, j], partner
        )

    def go(step, j):
        dispatch(step, j).start()
        return j

    lax.fori_loop(0, 8, go, 0)
    lax.fori_loop(0, 8, go, 1)

    def carry(k):
        return remote(
            cm, carries.at[k - 1], c_s.at[k - 1], c_r.at[k - 1], ((p + k) % 16, t)
        )

    def carry_go(k, _):
        carry(k).start()
        return 0

    lax.fori_loop(1, 16, carry_go, 0)

    wide = lambda at: pl.ds(pl.multiple_of(at * 2048, 2048), 2048)
    swaps = [
        remote(sh, sh2, p_s.at[0], p_r.at[0], partner),
        remote(op.at[:, wide(o)], o_pr.at[1], p_s.at[1], p_r.at[1], partner),
        remote(eg, w_in.at[:, 256:384], p_s.at[2], p_r.at[2], partner),
        remote(eu, w_in.at[:, 384:512], p_s.at[3], p_r.at[3], partner),
        remote(ed, w_dn.at[128:256], p_s.at[4], p_r.at[4], partner),
        remote(sd.at[:, wide(o)], s_dn.at[1], p_s.at[5], p_r.at[5], partner),
    ]
    owns = [
        pltpu.make_async_copy(op.at[:, wide(c)], o_pr.at[0], l_s.at[0]),
        pltpu.make_async_copy(eg, w_in.at[:, 0:128], l_s.at[1]),
        pltpu.make_async_copy(eu, w_in.at[:, 128:256], l_s.at[2]),
        pltpu.make_async_copy(ed, w_dn.at[0:128], l_s.at[3]),
        pltpu.make_async_copy(sd.at[:, wide(c)], s_dn.at[0], l_s.at[4]),
    ]
    for copy in swaps + owns:
        copy.start()

    def carry_in(k, _):
        carry(k).wait_recv()
        return 0

    lax.fori_loop(1, 16, carry_in, 0)

    def fold(n, state):
        k = 15 - n
        later = carries[k - 1]
        return jnp.where(k <= p, later[0:4] * state + later[4:8], state)

    state = lax.fori_loop(0, 15, fold, jnp.zeros((4, 128), jnp.float32))
    for j in range(4):
        cols = slice(128 * j, 128 * j + 128)
        states = loc[:, cols] + acum[:, cols] * state[j : j + 1]
        gts[0, :, cols] = (gate[:, cols] * states).astype(jnp.bfloat16)

    gswap = remote(gts.at[0], gts.at[1], p_s.at[6], p_r.at[6], partner)
    gswap.start()

    def forward(i, d):
        return remote(
            rows.at[y, i], rows.at[y, i], f_s.at[i, d], f_r.at[i, d],
            (p, 2 * ((y + 1 + 2 * d) % 4) + c),
        )

    def relay(step, _):
        i, copy = arrival(step, 0)
        copy.wait_recv()
        forward(i, 0).start()
        forward(i, 1).start()
        return 0

    lax.fori_loop(0, 8, relay, 0)

    def scatter(part, recv, send_sem, recv_sem, ch):
        return [
            remote(
                part.at[ch, (y + k) % 4], recv.at[ch, k - 1], send_sem.at[ch, k - 1],
                recv_sem.at[ch, k - 1], (p, 2 * ((y + k) % 4) + c),
            )
            for k in range(1, 4)
        ]

    def settle(part, recv, total, other, send_sem, recv_sem, base, ch):
        for copy in scatter(part, recv, send_sem, recv_sem, ch):
            copy.wait_recv()
        value = part[ch, y] + recv[ch, 0] + recv[ch, 1] + recv[ch, 2]
        total[ch] = value.reshape(2, 32, CW)
        swap(total, other, base, ch).start()

    def swap(total, other, base, ch):
        return remote(
            total.at[ch, o], other.at[ch], x_s.at[base + ch], x_r.at[base + ch], partner
        )

    def finish(total, other, scale, out, base):
        square = jnp.zeros((32, 1), jnp.float32)
        for ch in range(NCH):
            swap(total, other, base, ch).wait_recv()
            mine, theirs = total[ch, c], other[ch]
            square += jnp.sum(mine * mine + theirs * theirs, axis=1, keepdims=True)
        factor = lax.rsqrt(square / 4096.0 + eps)
        for ch in range(NCH):
            for values, side in ((total[ch, c], c), (other[ch], o)):
                cols = pl.ds(pl.multiple_of(side * 2048 + ch * CW, CW), CW)
                out[:, cols] = (values * factor * scale[:, cols]).astype(jnp.bfloat16)

    owns[0].wait()
    swaps[1].wait_recv()
    gswap.wait_recv()
    for ch in range(NCH):
        cols = slice(ch * CW, ch * CW + CW)
        m_part[ch] = (
            jnp.dot(gts[0], o_pr[0, :, cols], preferred_element_type=jnp.float32)
            + jnp.dot(gts[1], o_pr[1, :, cols], preferred_element_type=jnp.float32)
        ).reshape(4, 64, CW)
        for copy in scatter(m_part, m_recv, ms_s, ms_r, ch):
            copy.start()

    owns[4].wait()
    swaps[0].wait_recv()
    swaps[5].wait_recv()
    for ch in range(NCH):
        cols = slice(ch * CW, ch * CW + CW)
        e_part[ch] = (
            jnp.dot(sh[...], s_dn[0, :, cols], preferred_element_type=jnp.float32)
            + jnp.dot(sh2[...], s_dn[1, :, cols], preferred_element_type=jnp.float32)
        ).reshape(4, 64, CW)

    for copy in owns[1:4]:
        copy.wait()
    for copy in swaps[2:5]:
        copy.wait_recv()

    def landed(step, _):
        i, copy = arrival(step, 1)
        copy.wait_recv()
        for d in range(2):
            source = (y + 3 + 2 * d) % 4
            remote(
                rows.at[source, i], rows.at[source, i], f_s.at[i, d], f_r.at[i, d], partner
            ).wait_recv()
        return 0

    lax.fori_loop(0, 8, landed, 0)

    acc[...] = jnp.zeros_like(acc)

    def quarter(q, _):
        depth = pl.ds(pl.multiple_of(q * 1024, 1024), 1024)
        acc[...] += jnp.dot(
            rows[q].reshape(384, 1024), w_in[depth, :], preferred_element_type=jnp.float32
        )
        return 0

    lax.fori_loop(0, 4, quarter, 0)
    for side in range(2):
        g = acc[:, 256 * side : 256 * side + 128]
        u = acc[:, 256 * side + 128 : 256 * side + 256]
        hid[:, 128 * side : 128 * side + 128] = (
            g / (1.0 + jnp.exp(-g)) * u
        ).astype(jnp.bfloat16)

    def returning(ch, step, h):
        i = (half + step) % 8
        s = 2 * i + o
        return i, s, remote(
            res.at[ch, h, i], back.at[ch, p], r_s.at[ch, i, h], r_r.at[ch, p], (s, 2 * y + h)
        )

    def give(ch):
        for h in range(2):
            cols = slice(h * 2048 + ch * CW, h * 2048 + ch * CW + CW)
            res[ch, h] = (
                jnp.dot(hid[...], w_dn[:, cols], preferred_element_type=jnp.float32)
                .astype(jnp.bfloat16)
                .reshape(8, 48, CW)
            )

        def send(step, _):
            for h in range(2):
                i, s, copy = returning(ch, step, h)

                @pl.when(jnp.logical_or(s != p, c != h))
                def _():
                    copy.start()

                @pl.when(jnp.logical_and(s == p, c == h))
                def _():
                    back[ch, p] = res[ch, h, i]

            return 0

        lax.fori_loop(0, 8, send, 0)

    for ch in range(NCH):
        give(ch)

    for ch in range(NCH):
        settle(m_part, m_recv, m_sum, m_other, ms_s, ms_r, 0, ch)
    finish(m_sum, m_other, mscale, out_m, 0)

    for ch in range(NCH):

        def got(e, _):
            @pl.when(jnp.logical_or(e != p, c != 1 - par))
            def _():
                remote(
                    res.at[ch, 0, 0], back.at[ch, e], r_s.at[ch, 0, 0], r_r.at[ch, e], partner
                ).wait_recv()

            return 0

        lax.fori_loop(0, 16, got, 0)
        rows_back = back[ch].reshape(768, CW)
        e_part[ch] = e_part[ch] + (
            jnp.dot(whi[...], rows_back, preferred_element_type=jnp.float32)
            + jnp.dot(wlo[...], rows_back, preferred_element_type=jnp.float32)
        ).reshape(4, 64, CW)
        for copy in scatter(e_part, e_recv, es_s, es_r, ch):
            copy.start()

    for ch in range(NCH):
        settle(e_part, e_recv, e_sum, e_other, es_s, es_r, NCH, ch)
    finish(e_sum, e_other, escale, out_e, NCH)

    def drain(step, _):
        for j in range(2):
            dispatch(step, j).wait_send()
            forward(step, j).wait_send()
        for ch in range(NCH):
            for h in range(2):
                i, s, copy = returning(ch, step, h)

                @pl.when(jnp.logical_or(s != p, c != h))
                def _():
                    copy.wait_send()

        return 0

    lax.fori_loop(0, 8, drain, 0)

    def carry_out(k, _):
        carry(k).wait_send()
        return 0

    lax.fori_loop(1, 16, carry_out, 0)
    for copy in swaps:
        copy.wait_send()
    gswap.wait_send()
    for ch in range(NCH):
        for copy in scatter(m_part, m_recv, ms_s, ms_r, ch):
            copy.wait_send()
        for copy in scatter(e_part, e_recv, es_s, es_r, ch):
            copy.wait_send()
        swap(m_sum, m_other, 0, ch).wait_send()
        swap(e_sum, e_other, NCH, ch).wait_send()


def exchange(*operands):
    f32, bf16 = jnp.float32, jnp.bfloat16
    dma = pltpu.SemaphoreType.DMA
    hbm = pl.BlockSpec(memory_space=pltpu.HBM)
    vmem = pl.BlockSpec(memory_space=pltpu.VMEM)
    return pl.pallas_call(
        exchange_kernel,
        out_shape=[jax.ShapeDtypeStruct((32, 4096), bf16)] * 2,
        in_specs=[hbm] * 6 + [vmem] * 9,
        out_specs=[vmem] * 2,
        scratch_shapes=[
            pltpu.VMEM((4, 8, 48, 1024), bf16),
            pltpu.VMEM((4096, 512), bf16),
            pltpu.VMEM((256, 4096), bf16),
            pltpu.VMEM((2, 128, 2048), bf16),
            pltpu.VMEM((2, 512, 2048), bf16),
            pltpu.VMEM((256, 128), bf16),
            pltpu.VMEM((2, 256, 512), bf16),
            pltpu.VMEM((15, 8, 128), f32),
            pltpu.VMEM((384, 512), f32),
            pltpu.VMEM((384, 256), bf16),
            pltpu.VMEM((NCH, 2, 8, 48, CW), bf16),
            pltpu.VMEM((NCH, 16, 48, CW), bf16),
        ]
        + [
            pltpu.VMEM((NCH, 4, 64, CW), f32),
            pltpu.VMEM((NCH, 3, 64, CW), f32),
            pltpu.VMEM((NCH, 2, 32, CW), f32),
            pltpu.VMEM((NCH, 32, CW), f32),
        ]
        * 2
        + [
            dma((8, 2)), dma((8, 2)), dma((8, 2)), dma((8, 2)), dma((15,)), dma((15,)),
            dma((7,)), dma((7,)), dma((5,)), dma((NCH, 8, 2)), dma((NCH, 16)),
            dma((NCH, 3)), dma((NCH, 3)), dma((NCH, 3)), dma((NCH, 3)),
            dma((2 * NCH,)), dma((2 * NCH,)),
        ],
        compiler_params=pltpu.CompilerParams(
            collective_id=0, has_side_effects=True, vmem_limit_bytes=60 * 1024 * 1024
        ),
    )(*operands)


def body(
    mixer_rows,
    mixer_gain,
    gate_proj,
    input_proj,
    conv_taps,
    input_gates,
    decay_gates,
    decay_offset,
    out_proj,
    mixer_scale,
    expert_rows,
    expert_gain,
    route_ids,
    route_weights,
    expert_gate,
    expert_up,
    expert_down,
    shared_gate,
    shared_up,
    shared_down,
    expert_scale,
):
    row_count = mixer_rows.shape[0]
    normed = rms_scale(mixer_rows, mixer_gain).astype(jnp.bfloat16)
    gate_branch = jax.nn.gelu(jnp.dot(normed, gate_proj, preferred_element_type=jnp.float32))
    branch = jnp.dot(normed, input_proj, preferred_element_type=jnp.float32).astype(jnp.bfloat16)
    tap_count = conv_taps.shape[0]
    earlier_rows = shifted(branch[row_count - tap_count + 1 :], "ep", 1)
    padded = jnp.concatenate([earlier_rows, branch], axis=0)
    conv_sum = conv_taps[0] * padded[0:row_count].astype(jnp.float32)
    for tap_index in range(1, tap_count):
        conv_sum = conv_sum + conv_taps[tap_index] * padded[
            tap_index : tap_index + row_count
        ].astype(jnp.float32)
    conv_out = conv_sum.astype(jnp.bfloat16)
    block_rows = conv_out.reshape(row_count, input_gates.shape[0], input_gates.shape[1])
    input_gate = jax.nn.sigmoid(
        jnp.einsum("rbi,bij->rbj", block_rows, input_gates, preferred_element_type=jnp.float32)
    ).reshape(row_count, -1)
    decay_gate = jax.nn.sigmoid(
        jnp.einsum("rbi,bij->rbj", block_rows, decay_gates, preferred_element_type=jnp.float32)
    ).reshape(row_count, -1)
    log_decay = -lru_power * decay_gate * jax.nn.softplus(-decay_offset)
    positions = lax.axis_index("ep") * row_count + jnp.arange(row_count, dtype=jnp.int32)
    input_scale = jnp.where((positions == 0)[:, None], 1.0, jnp.sqrt(-jnp.expm1(2.0 * log_decay)))
    drive_term = input_scale * input_gate * conv_out.astype(jnp.float32)
    decay_rate = jnp.exp(log_decay)
    decay_product, local_states = lax.associative_scan(
        linear_pair, (decay_rate, drive_term), axis=0
    )
    carry_message = jnp.concatenate(
        [decay_product[-1].reshape(4, 128), local_states[-1].reshape(4, 128)], axis=0
    )
    tp_index = lax.axis_index("tp")
    y, c = (tp_index // 2, tp_index % 2)
    expert_normed = rms_scale(expert_rows, expert_gain).astype(jnp.bfloat16)
    capacity = 48
    slots = slots_of(route_ids, 16, capacity)
    every = jnp.arange(16 * capacity, dtype=jnp.int32)[None, :]
    mixing = jnp.where(slots[0] == every, route_weights[:, 0:1], 0.0) + jnp.where(
        slots[1] == every, route_weights[:, 1:2], 0.0
    )
    coarse = lax.reduce_precision(mixing, 8, 7)
    mix_high = coarse.astype(jnp.bfloat16)
    mix_low = (mixing - coarse).astype(jnp.bfloat16)
    line = jnp.arange(8 * capacity, dtype=jnp.int32)[None, :]
    owned = (2 * (line // capacity) + c) * capacity + line % capacity
    chosen = jnp.logical_or(slots[0] == owned, slots[1] == owned).astype(jnp.bfloat16)
    outgoing = jnp.stack(
        [
            lax.dot_general(
                chosen,
                lax.dynamic_slice_in_dim(expert_normed, ((y + 2 * j) % 4) * 1024, 1024, axis=1),
                (((0,), (0,)), ((), ())),
                preferred_element_type=jnp.float32,
            )
            .astype(jnp.bfloat16)
            .reshape(8, capacity, 1024)
            for j in range(2)
        ],
        axis=1,
    )
    shared_hidden = (
        jax.nn.silu(jnp.dot(expert_normed, shared_gate, preferred_element_type=jnp.float32))
        * jnp.dot(expert_normed, shared_up, preferred_element_type=jnp.float32)
    ).astype(jnp.bfloat16)
    return tuple(
        exchange(
            outgoing,
            expert_gate[0],
            expert_up[0],
            expert_down[0],
            shared_down,
            out_proj,
            shared_hidden,
            decay_product,
            local_states,
            gate_branch,
            carry_message,
            mix_high,
            mix_low,
            mixer_scale[None, :],
            expert_scale[None, :],
        )
    )


def solution(mesh):
    placed = (
        P("ep", None),
        P(),
        P(None, "tp"),
        P(None, "tp"),
        P(None, "tp"),
        P("tp", None, None),
        P("tp", None, None),
        P("tp"),
        P("tp", None),
        P(),
        P("ep", None),
        P(),
        P("ep", None),
        P("ep", None),
        P("ep", None, "tp"),
        P("ep", None, "tp"),
        P("ep", "tp", None),
        P(None, "tp"),
        P(None, "tp"),
        P("tp", None),
        P(),
    )
    return jax.shard_map(
        body,
        mesh=mesh,
        in_specs=placed,
        out_specs=(P(("ep", "tp"), None), P(("ep", "tp"), None)),
        check_vma=False,
    )
```

time: 265 us -> 167 us (0.63)
  the two profiles are of different devices: /device:TPU:1 before, /device:TPU:7 now
where the time goes in v1:
time: 167 us
  Pallas kernels  118 us (71%)
  matrix products  15.6 us (9%)
  other arithmetic  14.4 us (9%)
  local copies, waits for them, and re-layouts  13.9 us (8%)
  starting transfers between devices  3.46 us (2%)
    pallas_call x1, Pallas kernels, exchange(): pl.pallas_call(exchange_kernel, out_shape=[jax.ShapeDtypeStruct((32, 4096...  118 us
    slice x52, local copies, waits for them, and re-layouts, body(): lax.associative_scan(linear_pair, (decay_rate, drive_term), axis=0)  6.78 us
    dot_general x1, matrix products, body(): jnp.dot(normed, gate_proj, preferred_element_type=jnp.float32)  5.15 us
    unnamed x34, local copies, waits for them, and re-layouts  4.24 us
    dot_general x1, matrix products, body(): jnp.dot(normed, input_proj, preferred_element_type=jnp.float32)  3.64 us
    ppermute x1, starting transfers between devices, shifted(): return lax.ppermute(block, axis, route)  3.46 us
  transfers between devices with their start and end apart: 1, of which 0 were waited for; matrix products, arithmetic and copies ran while one was open for 11% of the time, Pallas kernels for 0%

profile of v1, /device:TPU:7, one launch (start us, length us, event | category | flops | bytes accessed | tf_op | source)
XLA Modules:
  0.0 166.8 jit_solution(5695106445315366793)
XLA Ops:
  0.6 0.0 copy-start
  0.6 0.0 copy-start.4
  0.7 2.2 %fusion.3 = f32[256]{0:T(256)S(1)} fusion(bf16[256,4096]{1,0:T(8,128)(2,1)} %param.21), kind=kLoop, calls=%fused_computation.7 | loop fusion | flops 3145472 | bytes 2098176 | tf_op jit(solution)/shard_map/reduce_sum | solution.py:20
  2.9 0.1 copy-done.4
  3.0 3.6 %convolution_convert_fusion.2 = bf16[256,512]{1,0:T(8,128)(2,1)S(1)} fusion(bf16[4096,512]{1,0:T(8,128)(2,1)} %param.24, bf16[256,4096]{1,0:T(8,128)(2,1)S(1)} %copy-done.4, f32[4096]{0:T(1024)} %param.22, f32[256]{0:T(256)S(1)} %add_rsqrt_fusion), kind=kOutput, calls=%fused_computation.21 | convolution fusion | flops 1078067200 | bytes 6571008 | tf_op jit(solution)/shard_map/dot_general | solution.py:425
  6.6 0.0 copy-done.13
  6.6 0.0 copy-start.8
  6.6 0.0 copy-start.7
  6.6 0.6 slice.362
  7.2 3.5 %collective-permute-start = (bf16[3,512]{1,0:T(4,128)(2,1)}, bf16[3,512]{1,0:T(4,128)(2,1)}, u32[]{:S(2)}, u32[]{:S(2)}) collective-permute-start(bf16[3,512]{1,0:T(4,128)(2,1)} %slice.362), channel_id=1, source_target_pairs={{0,8},{8,16},{16,24},{24,32},{32,40},{40,48},{48,56},{56,64},{64,7... | collective-permute-start | bytes 9224 | tf_op jit(solution)/shard_map/ppermute | solution.py:15
  10.8 0.0 copy-done.1
  10.8 0.5 fusion
  11.3 0.3 select_reduce_fusion.1
  11.6 2.2 %fusion.2 = bf16[256,4096]{1,0:T(8,128)(2,1)S(1)} fusion(bf16[256,4096]{1,0:T(8,128)(2,1)} %param.31, f32[4096]{0:T(1024)S(1)} %copy-done.7, f32[256]{0:T(256)S(1)} %add_rsqrt_fusion.1), kind=kLoop, calls=%fused_computation.6 | loop fusion | flops 4194304 | bytes 4211712 | tf_op jit(solution)/shard_map/convert_element_type | solution.py:455
  13.9 1.4 convolution_convert_fusion
  15.3 1.5 convolution_convert_fusion.1
  16.8 0.7 fusion.81
  17.5 0.6 fusion.77
  18.1 0.0 copy-done.11
  18.1 0.6 fusion.69
  18.7 5.1 %fusion.23.gate = f32[256,512]{1,0:T(8,128)} fusion(bf16[4096,512]{1,0:T(8,128)(2,1)} %param.23, bf16[256,4096]{1,0:T(8,128)(2,1)} %param.21, f32[4096]{0:T(1024)} %param.22, f32[256]{0:T(256)} %copy-done.13), kind=kOutput, calls=%fused_computation.38 | convolution fusion | flops 1078984704 | bytes 6833152 | tf_op jit(solution)/shard_map/dot_general | solution.py:424
  23.9 0.5 fusion.79
  24.4 0.0 copy-done.3
  24.4 1.3 pad_maximum_fusion.send_x
  25.8 1.3 fusion.12.sh
  27.1 1.8 %fusion.13 = (bf16[256,768]{1,0:T(8,128)(2,1)}, bf16[256,768]{1,0:T(8,128)(2,1)}) fusion(f32[256]{0:T(256)} %bitcast.65, s32[256]{0:T(256)S(1)} %bitcast.57, f32[256]{0:T(256)} %bitcast.64, s32[256]{0:T(256)S(1)} %bitcast.54), kind=kLoop, calls=%fused_computation.26 | loop fusion | flops 1769472 | bytes 790528 | tf_op jit(solution)/shard_map/convert_element_type | solution.py:464
  28.9 0.0 collective-permute-done
  28.9 0.0 copy-start.15
  29.0 1.0 add_convert_fusion
  30.0 1.3 fusion.11
  31.3 0.2 copy.32
  31.5 0.4 fusion.9
  31.9 0.2 copy.31
  32.1 0.1 copy-done.10
  32.2 0.4 convert_multiply_fusion.4
  32.6 1.6 slice.357
  34.2 0.3 slice.323
  34.5 1.4 slice.320
  35.9 0.3 slice.286
  36.3 0.3 slice.322
  36.6 1.4 slice.285
  38.0 1.0 multiply_add_fusion
  39.0 0.1 slice.326
  39.1 0.1 slice.325
  39.2 0.1 slice.289
  39.4 0.1 slice.288
  40.4 0.2 slice.355
  40.6 0.2 slice.318
  41.7 0.0 copy-start.5
  41.7 0.0 copy-start.6
  41.7 0.1 fusion.44
  42.1 0.6 copy-done.5
  42.7 0.1 copy-done.6
  42.8 0.1 fusion.32
  42.9 0.1 pad.128
  43.0 0.1 pad.129
  43.1 0.9 add.344.loc
  44.0 0.1 pad.112
  44.1 0.1 pad.113
  44.2 0.9 add.318.acum
  45.1 0.6 pad_maximum_fusion.16.cm
  45.7 117.8 %shard_map.212 = (bf16[32,4096]{1,0:T(8,128)(2,1)}, bf16[32,4096]{1,0:T(8,128)(2,1)}) custom-call(bf16[8,2,48,1024]{3,2,1,0:T(8,128)(2,1)} %pad_maximum_fusion.send_x, bf16[4096,128]{1,0:T(8,128)(2,1)} %bitcast.43, bf16[4096,128]{1,0:T(8,128)(2,1)} %bitcast.44, bf16[128,4096]{1,0:T(8,128)(2,1)} %bitcast.45, bf16[128,4096]{1,0:T(8,128)(2,1)} %sd.1, ...), custom_call_target="tpu_custom_call" | custom-call | tf_op jit(solution)/shard_map/pallas_call | solution.py:361
  163.5 1.7 %copy.44 = bf16[32,4096]{1,0:T(8,128)(2,1)} copy(bf16[32,4096]{1,0:T(8,128)(2,1)} %get-tuple-element.58) | data formatting | bytes 524288
  165.1 1.7 %copy.45 = bf16[32,4096]{1,0:T(8,128)(2,1)} copy(bf16[32,4096]{1,0:T(8,128)(2,1)} %get-tuple-element.59) | data formatting | bytes 524288
  (130 shorter events, 1.8 us)
Async XLA Ops:
  0.6 16.2 %copy-start = (bf16[4096,128]{1,0:T(8,128)(2,1)S(1)}, bf16[4096,128]{1,0:T(8,128)(2,1)}, u32[]{:S(2)}) copy-start(bf16[4096,128]{1,0:T(8,128)(2,1)} %param.38) | copy-start | bytes 3145732
  0.6 2.3 %copy-start.4 = (bf16[256,4096]{1,0:T(8,128)(2,1)S(1)}, bf16[256,4096]{1,0:T(8,128)(2,1)}, u32[]{:S(2)}) copy-start(bf16[256,4096]{1,0:T(8,128)(2,1)} %param.21) | copy-start | bytes 6291460
  3.0 3.7 %copy-start.13 = (f32[256]{0:T(256)}, f32[256]{0:T(256)S(1)}, u32[]{:S(2)}) copy-start(f32[256]{0:T(256)S(1)} %add_rsqrt_fusion) | copy-start | bytes 3076
  3.0 7.8 %copy-start.1 = (bf16[256,4096]{1,0:T(8,128)(2,1)S(1)}, bf16[256,4096]{1,0:T(8,128)(2,1)}, u32[]{:S(2)}) copy-start(bf16[256,4096]{1,0:T(8,128)(2,1)} %param.31) | copy-start | bytes 6291460
  6.6 4.7 %copy-start.8 = (s32[256,2]{0,1:T(2,128)S(1)}, s32[256,2]{0,1:T(2,128)}, u32[]{:S(2)}) copy-start(s32[256,2]{0,1:T(2,128)} %param.33) | copy-start | bytes 6148
  6.6 5.0 %copy-start.7 = (f32[4096]{0:T(1024)S(1)}, f32[4096]{0:T(1024)}, u32[]{:S(2)}) copy-start(f32[4096]{0:T(1024)} %param.32) | copy-start | bytes 49156
  7.2 21.7 %collective-permute-start = (bf16[3,512]{1,0:T(4,128)(2,1)}, bf16[3,512]{1,0:T(4,128)(2,1)}, u32[]{:S(2)}, u32[]{:S(2)}) collective-permute-start(bf16[3,512]{1,0:T(4,128)(2,1)} %slice.362), channel_id=1, source_target_pairs={{0,8},{8,16},{16,24},{24,32},{32,40},{40,48},{48,56},{56,64},{64,7... | collective-permute-start | bytes 9224 | tf_op jit(solution)/shard_map/ppermute | solution.py:15
  15.3 2.2 %copy-start.9 = (f32[4,512]{1,0:T(4,128)S(1)}, f32[4,512]{1,0:T(4,128)}, u32[]{:S(2)}) copy-start(f32[4,512]{1,0:T(4,128)} %param.25) | copy-start | bytes 24580
  15.3 2.8 %copy-start.11 = (f32[512]{0:T(512)S(1)}, f32[512]{0:T(512)}, u32[]{:S(2)}) copy-start(f32[512]{0:T(512)} %param.28) | copy-start | bytes 6148
  18.7 5.2 %copy-start.12 = (f32[256,2]{0,1:T(2,128)S(1)}, f32[256,2]{0,1:T(2,128)}, u32[]{:S(2)}) copy-start(f32[256,2]{0,1:T(2,128)} %param.34) | copy-start | bytes 6148
  18.7 5.7 %copy-start.2 = (bf16[384,1024]{1,0:T(8,128)(2,1)S(1)}, bf16[384,1024]{1,0:T(8,128)(2,1)}, u32[]{:S(2)}) copy-start(bf16[384,1024]{1,0:T(8,128)(2,1)} %convolution_convert_fusion) | copy-start | bytes 2359300
  18.7 5.7 %copy-start.3 = (bf16[384,1024]{1,0:T(8,128)(2,1)S(1)}, bf16[384,1024]{1,0:T(8,128)(2,1)}, u32[]{:S(2)}) copy-start(bf16[384,1024]{1,0:T(8,128)(2,1)} %convolution_convert_fusion.1) | copy-start | bytes 2359300
  23.9 1.9 %copy-start.14 = (bf16[4096,128]{1,0:T(8,128)(2,1)S(1)}, bf16[4096,128]{1,0:T(8,128)(2,1)}, u32[]{:S(2)}) copy-start(bf16[4096,128]{1,0:T(8,128)(2,1)} %param.39) | copy-start | bytes 3145732
  28.9 2.6 %copy-start.15 = (bf16[2,256,256]{2,1,0:T(8,128)(2,1)S(1)}, bf16[2,256,256]{2,1,0:T(8,128)(2,1)}, u32[]{:S(2)}) copy-start(bf16[2,256,256]{2,1,0:T(8,128)(2,1)} %param.27) | copy-start | bytes 786436
  31.5 0.7 copy-start.10
  41.7 1.0 copy-start.5
  41.7 1.0 copy-start.6

commit v2 on v1

v2 whole, which is shorter than its diff:
```python
import jax
import jax.numpy as jnp
from jax import lax
from jax.experimental import pallas as pl
from jax.experimental.pallas import tpu as pltpu
from jax.sharding import PartitionSpec as P

eps = 1e-06
lru_power = 8.0


MESH = pl.DeviceIdType.MESH
NCH = 4
CW = 2048 // NCH
FAR_EVEN = ((2, 2), (1, 2), (3, 2), (2, 0), (0, 2), (1, 0), (3, 0), (0, 0))
FAR_ODD = ((2, 1), (2, 3), (1, 1), (3, 3), (1, 3), (3, 1), (0, 1), (0, 3))


def remote(src, dst, send, recv, device):
    return pltpu.make_async_remote_copy(
        src_ref=src, dst_ref=dst, send_sem=send, recv_sem=recv, device_id=device, device_id_type=MESH
    )


def hop(step, even, core):
    dz = jnp.where(even, FAR_EVEN[step][0], FAR_ODD[step][0])
    dx = jnp.where(even, FAR_EVEN[step][1], FAR_ODD[step][1])
    return jnp.where(core == 0, dz, (4 - dz) % 4), jnp.where(core == 0, dx, (4 - dx) % 4)


def log1p_small(u):
    series = u * (1 - u * (1 / 2 - u * (1 / 3 - u * (1 / 4 - u * (1 / 5 - u * (1 / 6))))))
    return jnp.where(u < 0.05, series, jnp.log(1.0 + u))


def one_minus_exp(z):
    series = 1.0 + z * (1 / 7)
    for n in (6, 5, 4, 3, 2):
        series = 1.0 + z * series * (1 / n)
    return jnp.where(z > -0.5, -z * series, 1.0 - jnp.exp(z))


def sigmoid(v):
    return 1.0 / (1.0 + jnp.exp(-v))


def whole_kernel(
    m_rows, g_proj, i_proj, i_gates, d_gates, op, x_rows, eg, eu, ed, sg, su, sd,
    m_gain, taps, offset, mscale, x_gain, ids, weights, escale,
    out_m, out_e,
    nx, nm, proj, bgates, send_x, w_sh, br, halo, gate, acum, loc, cm, sh, mix_hi, mix_lo,
    rows, w_in, w_dn, s_dn, o_pr, sh2, gts, carries, acc, hid, res, back,
    m_part, m_recv, m_sum, m_other, e_part, e_recv, e_sum, e_other,
    d_s, d_r, f_s, f_r, c_s, c_r, p_s, p_r, l_s, r_s, r_r, ms_s, ms_r, es_s, es_r, x_s, x_r, h_s, h_r,
):
    f32, bf16 = jnp.float32, jnp.bfloat16
    p = lax.axis_index("ep")
    t = lax.axis_index("tp")
    y = t // 2
    c = t % 2
    o = 1 - c
    z = p // 4
    x = p % 4
    par = p % 2
    half = p // 2
    partner = (p, 2 * y + o)

    def dot(a, b):
        return jnp.dot(a, b, preferred_element_type=f32)

    barrier = pltpu.get_barrier_semaphore()

    def greet(k, _):
        other = (p * 2 + c + k) % 32
        pl.semaphore_signal(
            barrier, inc=1, device_id=(other // 2, 2 * y + other % 2), device_id_type=MESH
        )
        return 0

    lax.fori_loop(1, 32, greet, 0)
    for k in range(1, 4):
        pl.semaphore_signal(
            barrier, inc=1, device_id=(p, 2 * ((y + k) % 4) + c), device_id_type=MESH
        )

    def wide(at):
        return pl.ds(pl.multiple_of(at * 2048, 2048), 2048)

    def local(src, dst, n):
        return pltpu.make_async_copy(src, dst, l_s.at[n])

    first = [local(x_rows.at[:, 1024 * q : 1024 * q + 1024], nx.at[q], q) for q in range(4)]
    second = [local(m_rows, nm, 4), local(i_proj, proj.at[1], 5), local(g_proj, proj.at[0], 6)]
    gates_in = [local(i_gates, bgates.at[0], 7), local(d_gates, bgates.at[1], 8)]
    own_w = [
        local(eg, w_in.at[:, 0:128], 9),
        local(eu, w_in.at[:, 128:256], 10),
        local(ed, w_dn.at[0:128], 11),
    ]
    own_o = local(op.at[:, wide(c)], o_pr.at[0], 12)
    own_s = [
        local(sd.at[:, wide(c)], s_dn.at[0], 13),
        local(sg, w_sh.at[:, 0:128], 14),
        local(su, w_sh.at[:, 128:256], 15),
    ]
    for copy in first:
        copy.start()

    id0, id1 = ids[0:1, :], ids[1:2, :]
    expert = lax.broadcasted_iota(jnp.int32, (16, 256), 0)
    named0, named1 = id0 == expert, id1 == expert
    either = jnp.where(jnp.logical_or(named0, named1), 1.0, 0.0).astype(bf16)
    ahead = jnp.where(
        lax.broadcasted_iota(jnp.int32, (256, 256), 0) < lax.broadcasted_iota(jnp.int32, (256, 256), 1),
        1.0,
        0.0,
    ).astype(bf16)
    place = dot(either, ahead)
    slot0 = id0.astype(f32) * 48.0 + jnp.sum(jnp.where(named0, place, 0.0), axis=0, keepdims=True)
    slot1 = id1.astype(f32) * 48.0 + jnp.sum(jnp.where(named1, place, 0.0), axis=0, keepdims=True)

    def picked(i):
        line = ((2 * i + c) * 48 + lax.broadcasted_iota(jnp.int32, (48, 256), 0)).astype(f32)
        return jnp.where(jnp.logical_or(slot0 == line, slot1 == line), 1.0, 0.0).astype(bf16)

    chosen = jnp.concatenate([picked(i) for i in range(8)], axis=0)

    for copy in first:
        copy.wait()
    for copy in second + gates_in:
        copy.start()

    def norm_x(r, _):
        at = pl.ds(pl.multiple_of(r * 32, 32), 32)
        parts = [nx[q, at, :].astype(f32) for q in range(4)]
        square = sum(jnp.sum(v * v, axis=1, keepdims=True) for v in parts)
        factor = lax.rsqrt(square / 4096.0 + eps)
        for q in range(4):
            nx[q, at, :] = (parts[q] * factor * x_gain[:, 1024 * q : 1024 * q + 1024]).astype(bf16)
        return 0

    lax.fori_loop(0, 8, norm_x, 0)
    for j in range(2):
        send_x[j] = dot(chosen, nx[(y + 2 * j) % 4]).astype(bf16).reshape(8, 48, 1024)

    pl.semaphore_wait(barrier, 34)

    def dispatch(step, j):
        dz, dx = hop(step, par == c, c)
        e = ((z + dz) % 4) * 4 + (x + dx) % 4
        return remote(
            send_x.at[j, e // 2], rows.at[(y + 2 * j) % 4, half], d_s.at[step, j],
            d_r.at[half, j], (e, 2 * y + 1 - par),
        )

    def arrival(step, j):
        dz, dx = hop(step, par == o, par)
        i = (((z + 4 - dz) % 4) * 4 + (x + 4 - dx) % 4) // 2
        return i, remote(send_x.at[j, i], rows.at[(y + 2 * j) % 4, i], d_s.at[step, j], d_r.at[i, j], partner)

    for j in range(2):
        for step in range(8):
            dispatch(step, j).start()

    swaps = [
        remote(sh, sh2, p_s.at[0], p_r.at[0], partner),
        remote(op.at[:, wide(o)], o_pr.at[1], p_s.at[1], p_r.at[1], partner),
        remote(eg, w_in.at[:, 256:384], p_s.at[2], p_r.at[2], partner),
        remote(eu, w_in.at[:, 384:512], p_s.at[3], p_r.at[3], partner),
        remote(ed, w_dn.at[128:256], p_s.at[4], p_r.at[4], partner),
        remote(sd.at[:, wide(o)], s_dn.at[1], p_s.at[5], p_r.at[5], partner),
        remote(gts.at[0], gts.at[1], p_s.at[6], p_r.at[6], partner),
    ]
    for copy in swaps[2:5] + own_w + [swaps[1], own_o, swaps[5]] + own_s:
        copy.start()

    def forward(i, d):
        return remote(
            rows.at[y, i], rows.at[y, i], f_s.at[i, d], f_r.at[i, d],
            (p, 2 * ((y + 1 + 2 * d) % 4) + c),
        )

    def relay(step):
        i, copy = arrival(step, 0)
        copy.wait_recv()
        forward(i, 0).start()
        forward(i, 1).start()

    second[0].wait()

    def norm_m(r, _):
        at = pl.ds(pl.multiple_of(r * 32, 32), 32)
        v = nm[at, :].astype(f32)
        factor = lax.rsqrt(jnp.sum(v * v, axis=1, keepdims=True) / 4096.0 + eps)
        nm[at, :] = (v * factor * m_gain[...]).astype(bf16)
        return 0

    lax.fori_loop(0, 8, norm_m, 0)
    second[1].wait()

    def project(n, _):
        cols = pl.ds(pl.multiple_of(n * 256, 256), 256)
        br[:, cols] = dot(nm[...], proj[1, :, cols]).astype(bf16)
        return 0

    lax.fori_loop(0, 2, project, 0)
    give_halo = remote(br.at[240:256], halo, h_s.at[0], h_r.at[0], ((p + 1) % 16, t))
    give_halo.start()
    relay(0)
    relay(1)
    second[2].wait()

    def gates(n, _):
        cols = pl.ds(pl.multiple_of(n * 256, 256), 256)
        v = dot(nm[...], proj[0, :, cols])
        gate[:, cols] = 0.5 * v * (1.0 + jnp.tanh(0.7978845608028654 * (v + 0.044715 * (v * v * v))))
        return 0

    lax.fori_loop(0, 2, gates, 0)
    relay(2)
    relay(3)
    for copy in gates_in:
        copy.wait()
    give_halo.wait_recv()

    row = lax.broadcasted_iota(jnp.int32, (256, 128), 0)

    def recur(b, _):
        cols = pl.ds(pl.multiple_of(b * 256, 256), 256)
        before = jnp.where(p == 0, 0.0, halo[:, cols].astype(f32))
        ext = jnp.concatenate([before, br[:, cols].astype(f32)], axis=0)
        tap = taps[:, cols]
        conv = tap[0:1] * pltpu.roll(ext, 3, 0)[16:]
        for k in range(1, 4):
            conv = conv + tap[k : k + 1] * (pltpu.roll(ext, 3 - k, 0) if k < 3 else ext)[16:]
        conv_out = conv.astype(bf16)
        gi = sigmoid(dot(conv_out, bgates[0, b]))
        gd = sigmoid(dot(conv_out, bgates[1, b]))
        off = offset[:, cols]
        soft = jnp.maximum(-off, 0.0) + log1p_small(jnp.exp(-jnp.abs(off)))
        log_decay = -lru_power * gd * soft
        scale = jnp.sqrt(one_minus_exp(2.0 * log_decay))
        first_row = jnp.logical_and(lax.broadcasted_iota(jnp.int32, (256, 256), 0) == 0, p == 0)
        scale = jnp.where(first_row, 1.0, scale)
        loc[:, cols] = scale * gi * conv_out.astype(f32)
        acum[:, cols] = jnp.exp(log_decay)
        return 0

    lax.fori_loop(0, 2, recur, 0)
    relay(4)
    relay(5)

    def scan(b, _):
        cols = pl.ds(pl.multiple_of(b * 128, 128), 128)
        av, bv = acum[:, cols], loc[:, cols]
        for d in (1, 2, 4, 8, 16, 32, 64, 128):
            if d < 8:
                a_up = jnp.where(row < d, 1.0, pltpu.roll(av, d, 0))
                b_up = jnp.where(row < d, 0.0, pltpu.roll(bv, d, 0))
            else:
                a_up = jnp.concatenate([jnp.ones((d, 128), f32), av[: 256 - d]], axis=0)
                b_up = jnp.concatenate([jnp.zeros((d, 128), f32), bv[: 256 - d]], axis=0)
            bv = av * b_up + bv
            av = av * a_up
        acum[:, cols] = av
        loc[:, cols] = bv
        cm[pl.ds(b, 1), :] = av[255:256]
        cm[pl.ds(4 + b, 1), :] = bv[255:256]
        return 0

    lax.fori_loop(0, 4, scan, 0)

    def carry(k):
        return remote(cm, carries.at[k - 1], c_s.at[k - 1], c_r.at[k - 1], ((p + k) % 16, t))

    relay(6)
    relay(7)

    def carry_go(k, _):
        carry(k).start()
        return 0

    lax.fori_loop(1, 16, carry_go, 0)

    line = lax.broadcasted_iota(jnp.int32, (128, 256), 0)
    tile = jnp.where(
        line == 0, slot0,
        jnp.where(line == 1, slot1, jnp.where(line == 2, weights[0:1, :], jnp.where(line == 3, weights[1:2, :], 0.0))),
    )
    turned = tile.T
    every = lax.broadcasted_iota(jnp.int32, (256, 768), 1).astype(f32)
    mixing = jnp.where(turned[:, 0:1] == every, turned[:, 2:3], 0.0) + jnp.where(
        turned[:, 1:2] == every, turned[:, 3:4], 0.0
    )
    high = mixing.astype(bf16)
    mix_hi[...] = high
    mix_lo[...] = (mixing - high.astype(f32)).astype(bf16)

    for copy in own_w:
        copy.wait()
    for copy in swaps[2:5]:
        copy.wait_recv()
    for step in range(8):
        i, copy = arrival(step, 1)
        copy.wait_recv()
        for d in range(2):
            source = (y + 3 + 2 * d) % 4
            remote(
                rows.at[source, i], rows.at[source, i], f_s.at[i, d], f_r.at[i, d], partner
            ).wait_recv()

    acc[...] = jnp.zeros_like(acc)

    def quarter(q, _):
        depth = pl.ds(pl.multiple_of(q * 1024, 1024), 1024)
        acc[...] += dot(rows[q].reshape(384, 1024), w_in[depth, :])
        return 0

    lax.fori_loop(0, 4, quarter, 0)
    for side in range(2):
        g = acc[:, 256 * side : 256 * side + 128]
        u = acc[:, 256 * side + 128 : 256 * side + 256]
        hid[:, 128 * side : 128 * side + 128] = (g / (1.0 + jnp.exp(-g)) * u).astype(bf16)

    def returning(ch, step, h):
        dz, dx = hop(step, par == o, c)
        s = ((z + dz) % 4) * 4 + (x + dx) % 4
        return s // 2, s, remote(
            res.at[ch, h, s // 2], back.at[ch, p], r_s.at[ch, step, h], r_r.at[ch, p], (s, 2 * y + h)
        )

    def give(ch, _):
        for h in range(2):
            cols = pl.ds(pl.multiple_of(h * 2048 + ch * CW, CW), CW)
            res[ch, h] = dot(hid[...], w_dn[:, cols]).astype(bf16).reshape(8, 48, CW)
        for h in range(2):
            for step in range(8):
                i, s, copy = returning(ch, step, h)
                if step < 7:
                    copy.start()
                else:

                    @pl.when(jnp.logical_or(s != p, c != h))
                    def _():
                        copy.start()

                    @pl.when(jnp.logical_and(s == p, c == h))
                    def _():
                        back[ch, p] = res[ch, h, i]

        return 0

    lax.fori_loop(0, NCH, give, 0)

    def carry_in(k, _):
        carry(k).wait_recv()
        return 0

    lax.fori_loop(1, 16, carry_in, 0)

    def fold(n, state):
        k = 15 - n
        later = carries[k - 1]
        return jnp.where(k <= p, later[0:4] * state + later[4:8], state)

    state = lax.fori_loop(0, 15, fold, jnp.zeros((4, 128), f32))
    for j in range(4):
        cols = slice(128 * j, 128 * j + 128)
        states = loc[:, cols] + acum[:, cols] * state[j : j + 1]
        gts[0, :, cols] = (gate[:, cols] * states).astype(bf16)

    for copy in own_s:
        copy.wait()
    shared = dot(nx[0], w_sh[0:1024, :])
    for q in range(1, 4):
        shared = shared + dot(nx[q], w_sh[1024 * q : 1024 * q + 1024, :])
    g, u = shared[:, 0:128], shared[:, 128:256]
    swaps[6].start()
    sh[...] = (g / (1.0 + jnp.exp(-g)) * u).astype(bf16)
    own_o.wait()
    swaps[1].wait_recv()
    swaps[6].wait_recv()
    swaps[0].start()

    def scatter(part, recv, send_sem, recv_sem, ch):
        return [
            remote(
                part.at[ch, (y + k) % 4], recv.at[ch, k - 1], send_sem.at[ch, k - 1],
                recv_sem.at[ch, k - 1], (p, 2 * ((y + k) % 4) + c),
            )
            for k in range(1, 4)
        ]

    def swap(total, other, base, ch):
        return remote(
            total.at[ch, o], other.at[ch], x_s.at[base + ch], x_r.at[base + ch], partner
        )

    def settle(part, recv, total, other, send_sem, recv_sem, base):
        def one(ch, _):
            for copy in scatter(part, recv, send_sem, recv_sem, ch):
                copy.wait_recv()
            value = part[ch, y] + recv[ch, 0] + recv[ch, 1] + recv[ch, 2]
            total[ch] = value.reshape(2, 32, CW)
            swap(total, other, base, ch).start()
            return 0

        lax.fori_loop(0, NCH, one, 0)

    def finish(total, other, scale, out, base):
        square = jnp.zeros((32, 1), f32)
        for ch in range(NCH):
            swap(total, other, base, ch).wait_recv()
            mine, theirs = total[ch, c], other[ch]
            square += jnp.sum(mine * mine + theirs * theirs, axis=1, keepdims=True)
        factor = lax.rsqrt(square / 4096.0 + eps)
        for ch in range(NCH):
            for values, side in ((total[ch, c], c), (other[ch], o)):
                cols = pl.ds(pl.multiple_of(side * 2048 + ch * CW, CW), CW)
                out[:, cols] = (values * factor * scale[:, cols]).astype(bf16)

    def mixed(ch, _):
        cols = pl.ds(pl.multiple_of(ch * CW, CW), CW)
        m_part[ch] = (dot(gts[0], o_pr[0, :, cols]) + dot(gts[1], o_pr[1, :, cols])).reshape(4, 64, CW)
        for copy in scatter(m_part, m_recv, ms_s, ms_r, ch):
            copy.start()
        return 0

    lax.fori_loop(0, NCH, mixed, 0)

    swaps[0].wait_recv()
    swaps[5].wait_recv()

    def shared_part(ch, _):
        cols = pl.ds(pl.multiple_of(ch * CW, CW), CW)
        e_part[ch] = (dot(sh[...], s_dn[0, :, cols]) + dot(sh2[...], s_dn[1, :, cols])).reshape(4, 64, CW)
        return 0

    lax.fori_loop(0, NCH, shared_part, 0)

    def combine(ch, _):
        def got(e, _):
            @pl.when(jnp.logical_or(e != p, c != 1 - par))
            def _():
                remote(
                    res.at[ch, 0, 0], back.at[ch, e], r_s.at[ch, 0, 0], r_r.at[ch, e], partner
                ).wait_recv()

            return 0

        lax.fori_loop(0, 16, got, 0)
        returned = back[ch].reshape(768, CW)
        e_part[ch] = e_part[ch] + (
            dot(mix_hi[...], returned) + dot(mix_lo[...], returned)
        ).reshape(4, 64, CW)
        for copy in scatter(e_part, e_recv, es_s, es_r, ch):
            copy.start()
        return 0

    lax.fori_loop(0, NCH - 1, combine, 0)
    settle(m_part, m_recv, m_sum, m_other, ms_s, ms_r, 0)
    finish(m_sum, m_other, mscale, out_m, 0)
    combine(NCH - 1, 0)
    settle(e_part, e_recv, e_sum, e_other, es_s, es_r, NCH)
    finish(e_sum, e_other, escale, out_e, NCH)

    for step in range(8):
        for j in range(2):
            dispatch(step, j).wait_send()
            forward(step, j).wait_send()

    def drain(ch, _):
        for step in range(8):
            for h in range(2):
                i, s, copy = returning(ch, step, h)
                if step < 7:
                    copy.wait_send()
                else:

                    @pl.when(jnp.logical_or(s != p, c != h))
                    def _():
                        copy.wait_send()

        for copy in scatter(m_part, m_recv, ms_s, ms_r, ch):
            copy.wait_send()
        for copy in scatter(e_part, e_recv, es_s, es_r, ch):
            copy.wait_send()
        swap(m_sum, m_other, 0, ch).wait_send()
        swap(e_sum, e_other, NCH, ch).wait_send()
        return 0

    lax.fori_loop(0, NCH, drain, 0)

    def carry_out(k, _):
        carry(k).wait_send()
        return 0

    lax.fori_loop(1, 16, carry_out, 0)
    for copy in swaps:
        copy.wait_send()
    give_halo.wait_send()


def body(
    mixer_rows, mixer_gain, gate_proj, input_proj, conv_taps, input_gates, decay_gates,
    decay_offset, out_proj, mixer_scale, expert_rows, expert_gain, route_ids, route_weights,
    expert_gate, expert_up, expert_down, shared_gate, shared_up, shared_down, expert_scale,
):
    f32, bf16 = jnp.float32, jnp.bfloat16
    dma = pltpu.SemaphoreType.DMA
    hbm = pl.BlockSpec(memory_space=pltpu.HBM)
    vmem = pl.BlockSpec(memory_space=pltpu.VMEM)
    outs = pl.pallas_call(
        whole_kernel,
        out_shape=[jax.ShapeDtypeStruct((32, 4096), bf16)] * 2,
        in_specs=[hbm] * 13 + [vmem] * 8,
        out_specs=[vmem] * 2,
        scratch_shapes=[
            pltpu.VMEM((4, 256, 1024), bf16),
            pltpu.VMEM((256, 4096), bf16),
            pltpu.VMEM((2, 4096, 512), bf16),
            pltpu.VMEM((2, 2, 256, 256), bf16),
            pltpu.VMEM((2, 8, 48, 1024), bf16),
            pltpu.VMEM((4096, 256), bf16),
            pltpu.VMEM((256, 512), bf16),
            pltpu.VMEM((16, 512), bf16),
            pltpu.VMEM((256, 512), f32),
            pltpu.VMEM((256, 512), f32),
            pltpu.VMEM((256, 512), f32),
            pltpu.VMEM((8, 128), f32),
            pltpu.VMEM((256, 128), bf16),
            pltpu.VMEM((256, 768), bf16),
            pltpu.VMEM((256, 768), bf16),
            pltpu.VMEM((4, 8, 48, 1024), bf16),
            pltpu.VMEM((4096, 512), bf16),
            pltpu.VMEM((256, 4096), bf16),
            pltpu.VMEM((2, 128, 2048), bf16),
            pltpu.VMEM((2, 512, 2048), bf16),
            pltpu.VMEM((256, 128), bf16),
            pltpu.VMEM((2, 256, 512), bf16),
            pltpu.VMEM((15, 8, 128), f32),
            pltpu.VMEM((384, 512), f32),
            pltpu.VMEM((384, 256), bf16),
            pltpu.VMEM((NCH, 2, 8, 48, CW), bf16),
            pltpu.VMEM((NCH, 16, 48, CW), bf16),
        ]
        + [
            pltpu.VMEM((NCH, 4, 64, CW), f32),
            pltpu.VMEM((NCH, 3, 64, CW), f32),
            pltpu.VMEM((NCH, 2, 32, CW), f32),
            pltpu.VMEM((NCH, 32, CW), f32),
        ]
        * 2
        + [
            dma((8, 2)), dma((8, 2)), dma((8, 2)), dma((8, 2)), dma((15,)), dma((15,)),
            dma((7,)), dma((7,)), dma((16,)), dma((NCH, 8, 2)), dma((NCH, 16)),
            dma((NCH, 3)), dma((NCH, 3)), dma((NCH, 3)), dma((NCH, 3)),
            dma((2 * NCH,)), dma((2 * NCH,)), dma((1,)), dma((1,)),
        ],
        compiler_params=pltpu.CompilerParams(
            collective_id=0, has_side_effects=True, vmem_limit_bytes=67043328
        ),
    )(
        mixer_rows, gate_proj, input_proj, input_gates, decay_gates, out_proj, expert_rows,
        expert_gate[0], expert_up[0], expert_down[0], shared_gate, shared_up, shared_down,
        mixer_gain[None, :], conv_taps, decay_offset[None, :], mixer_scale[None, :],
        expert_gain[None, :], route_ids.T, route_weights.T, expert_scale[None, :],
    )
    return tuple(outs)


def solution(mesh):
    placed = (
        P("ep", None),
        P(),
        P(None, "tp"),
        P(None, "tp"),
        P(None, "tp"),
        P("tp", None, None),
        P("tp", None, None),
        P("tp"),
        P("tp", None),
        P(),
        P("ep", None),
        P(),
        P("ep", None),
        P("ep", None),
        P("ep", None, "tp"),
        P("ep", None, "tp"),
        P("ep", "tp", None),
        P(None, "tp"),
        P(None, "tp"),
        P("tp", None),
        P(),
    )
    return jax.shard_map(
        body,
        mesh=mesh,
        in_specs=placed,
        out_specs=(P(("ep", "tp"), None), P(("ep", "tp"), None)),
        check_vma=False,
    )
```

time: 167 us -> 104 us (0.62)
  the two profiles are of different devices: /device:TPU:7 before, /device:TPU:1 now
where the time goes in v2:
time: 104 us
  Pallas kernels  100 us (96%)
  local copies, waits for them, and re-layouts  3.34 us (3%)
    pallas_call x1, Pallas kernels, body(): pl.pallas_call(whole_kernel, out_shape=[jax.ShapeDtypeStruct((32, 4096),...  100 us
    unnamed x2, local copies, waits for them, and re-layouts  3.34 us

profile of v2, /device:TPU:1, one launch (start us, length us, event | category | flops | bytes accessed | tf_op | source)
XLA Modules:
  0.0 104.2 jit_solution(10674860872526004077)
XLA Ops:
  0.6 100.2 %shard_map.212 = (bf16[32,4096]{1,0:T(8,128)(2,1)}, bf16[32,4096]{1,0:T(8,128)(2,1)}) custom-call(bf16[256,4096]{1,0:T(8,128)(2,1)} %m_rows.1, bf16[4096,512]{1,0:T(8,128)(2,1)} %g_proj.1, bf16[4096,512]{1,0:T(8,128)(2,1)} %i_proj.1, bf16[2,256,256]{2,1,0:T(8,128)(2,1)} %i_gates.1, bf16[2,256,256]{2,1,0:T(8,128)(2,1)} %d_gates.1, bf16[512,4096]{1,0:T(8,128)(2,1)} %op.1, ...), custom_call_target="tpu_custom_call" | custom-call | tf_op jit(solution)/shard_map/pallas_call | solution.py:513
  100.9 1.7 %copy.25 = bf16[32,4096]{1,0:T(8,128)(2,1)} copy(bf16[32,4096]{1,0:T(8,128)(2,1)} %get-tuple-element.4) | data formatting | bytes 524288
  102.5 1.7 %copy.26 = bf16[32,4096]{1,0:T(8,128)(2,1)} copy(bf16[32,4096]{1,0:T(8,128)(2,1)} %get-tuple-element.5) | data formatting | bytes 524288

commit v3 on v2

--- a/solution.py
+++ b/solution.py
@@ -10,7 +10,9 @@
 
 
 MESH = pl.DeviceIdType.MESH
-NCH = 4
+NCH = 8
+FAR = 6
+ORDER0 = (5, 4, 3, 2, 1, 0)
 CW = 2048 // NCH
 FAR_EVEN = ((2, 2), (1, 2), (3, 2), (2, 0), (0, 2), (1, 0), (3, 0), (0, 0))
 FAR_ODD = ((2, 1), (2, 3), (1, 1), (3, 3), (1, 3), (3, 1), (0, 1), (0, 3))
@@ -46,11 +48,12 @@
 
 def whole_kernel(
     m_rows, g_proj, i_proj, i_gates, d_gates, op, x_rows, eg, eu, ed, sg, su, sd,
+    m_gain_h, taps_h, offset_h, mscale_h, x_gain_h, ids_h, weights_h, escale_h,
+    out_m, out_e,
     m_gain, taps, offset, mscale, x_gain, ids, weights, escale,
-    out_m, out_e,
-    nx, nm, proj, bgates, send_x, w_sh, br, halo, gate, acum, loc, cm, sh, mix_hi, mix_lo,
+    nx, nm, proj, bgates, send_x, send_n, w_sh, br, tail, edge, halo, gate, acum, loc, cm, sh, mix_hi, mix_lo,
     rows, w_in, w_dn, s_dn, o_pr, sh2, gts, carries, acc, hid, res, back,
-    m_part, m_recv, m_sum, m_other, e_part, e_recv, e_sum, e_other,
+    m_part, m_send, m_recv, m_sum, m_other, e_part, e_recv, e_sum, e_other,
     d_s, d_r, f_s, f_r, c_s, c_r, p_s, p_r, l_s, r_s, r_r, ms_s, ms_r, es_s, es_r, x_s, x_r, h_s, h_r,
 ):
     f32, bf16 = jnp.float32, jnp.bfloat16
@@ -89,8 +92,9 @@
     def local(src, dst, n):
         return pltpu.make_async_copy(src, dst, l_s.at[n])
 
+    early = [local(m_rows.at[240:256], tail, 16), local(i_proj, proj.at[1], 5)]
     first = [local(x_rows.at[:, 1024 * q : 1024 * q + 1024], nx.at[q], q) for q in range(4)]
-    second = [local(m_rows, nm, 4), local(i_proj, proj.at[1], 5), local(g_proj, proj.at[0], 6)]
+    second = [local(m_rows, nm, 4), local(g_proj, proj.at[0], 6)]
     gates_in = [local(i_gates, bgates.at[0], 7), local(d_gates, bgates.at[1], 8)]
     own_w = [
         local(eg, w_in.at[:, 0:128], 9),
@@ -103,8 +107,12 @@
         local(sg, w_sh.at[:, 0:128], 14),
         local(su, w_sh.at[:, 128:256], 15),
     ]
-    for copy in first:
+    small = [local(ids_h, ids, 17), local(weights_h, weights, 18), local(x_gain_h, x_gain, 19)]
+    small += [local(m_gain_h, m_gain, 20), local(taps_h, taps, 21), local(offset_h, offset, 22)]
+    small += [local(mscale_h, mscale, 23), local(escale_h, escale, 24)]
+    for copy in small[:1] + first + small[1:]:
         copy.start()
+    small[0].wait()
 
     id0, id1 = ids[0:1, :], ids[1:2, :]
     expert = lax.broadcasted_iota(jnp.int32, (16, 256), 0)
@@ -125,9 +133,9 @@
 
     chosen = jnp.concatenate([picked(i) for i in range(8)], axis=0)
 
-    for copy in first:
+    for copy in first + small[1:]:
         copy.wait()
-    for copy in second + gates_in:
+    for copy in early + second + gates_in:
         copy.start()
 
     def norm_x(r, _):
@@ -142,25 +150,45 @@
     lax.fori_loop(0, 8, norm_x, 0)
     for j in range(2):
         send_x[j] = dot(chosen, nx[(y + 2 * j) % 4]).astype(bf16).reshape(8, 48, 1024)
+    near = []
+    for step in range(FAR, 8):
+        dz, dx = hop(step, par == c, c)
+        near.append(((((z + dz) % 4) * 4 + (x + dx) % 4) // 2))
+    near_chosen = jnp.concatenate([picked(i) for i in near], axis=0)
+    for j in range(2):
+        send_n[j] = dot(near_chosen, nx[(y + 1 + 2 * j) % 4]).astype(bf16).reshape(8 - FAR, 48, 1024)
+
+    for copy in early:
+        copy.wait()
+    v = tail[...].astype(f32)
+    factor = lax.rsqrt(jnp.sum(v * v, axis=1, keepdims=True) / 4096.0 + eps)
+    last_rows = (v * factor * m_gain[...]).astype(bf16)
+    edge[...] = dot(last_rows, proj[1]).astype(bf16)
 
     pl.semaphore_wait(barrier, 34)
+    give_halo = remote(edge, halo, h_s.at[0], h_r.at[0], ((p + 1) % 16, t))
+    give_halo.start()
 
     def dispatch(step, j):
         dz, dx = hop(step, par == c, c)
         e = ((z + dz) % 4) * 4 + (x + dx) % 4
+        source = send_x.at[j, e // 2] if j < 2 else send_n.at[j - 2, step - FAR]
+        shift = (0, 2, 1, 3)[j]
         return remote(
-            send_x.at[j, e // 2], rows.at[(y + 2 * j) % 4, half], d_s.at[step, j],
-            d_r.at[half, j], (e, 2 * y + 1 - par),
+            source, rows.at[(y + shift) % 4, step], d_s.at[step, j], d_r.at[step, j],
+            (e, 2 * y + 1 - par),
         )
 
     def arrival(step, j):
-        dz, dx = hop(step, par == o, par)
-        i = (((z + 4 - dz) % 4) * 4 + (x + 4 - dx) % 4) // 2
-        return i, remote(send_x.at[j, i], rows.at[(y + 2 * j) % 4, i], d_s.at[step, j], d_r.at[i, j], partner)
-
-    for j in range(2):
-        for step in range(8):
-            dispatch(step, j).start()
+        shift = (0, 2, 1, 3)[j]
+        return remote(
+            send_x.at[0, 0], rows.at[(y + shift) % 4, step], d_s.at[step, j], d_r.at[step, j], partner
+        )
+
+    order = [(step, 0) for step in ORDER0] + [(step, 1) for step in range(8)]
+    order += [(step, j) for step in range(FAR, 8) for j in (0, 2, 3)]
+    for step, j in order:
+        dispatch(step, j).start()
 
     swaps = [
         remote(sh, sh2, p_s.at[0], p_r.at[0], partner),
@@ -181,10 +209,9 @@
         )
 
     def relay(step):
-        i, copy = arrival(step, 0)
-        copy.wait_recv()
-        forward(i, 0).start()
-        forward(i, 1).start()
+        arrival(step, 0).wait_recv()
+        forward(step, 0).start()
+        forward(step, 1).start()
 
     second[0].wait()
 
@@ -196,7 +223,6 @@
         return 0
 
     lax.fori_loop(0, 8, norm_m, 0)
-    second[1].wait()
 
     def project(n, _):
         cols = pl.ds(pl.multiple_of(n * 256, 256), 256)
@@ -204,11 +230,7 @@
         return 0
 
     lax.fori_loop(0, 2, project, 0)
-    give_halo = remote(br.at[240:256], halo, h_s.at[0], h_r.at[0], ((p + 1) % 16, t))
-    give_halo.start()
-    relay(0)
-    relay(1)
-    second[2].wait()
+    second[1].wait()
 
     def gates(n, _):
         cols = pl.ds(pl.multiple_of(n * 256, 256), 256)
@@ -217,8 +239,6 @@
         return 0
 
     lax.fori_loop(0, 2, gates, 0)
-    relay(2)
-    relay(3)
     for copy in gates_in:
         copy.wait()
     give_halo.wait_recv()
@@ -246,9 +266,14 @@
         acum[:, cols] = jnp.exp(log_decay)
         return 0
 
-    lax.fori_loop(0, 2, recur, 0)
-    relay(4)
-    relay(5)
+    for step in ORDER0[:2]:
+        relay(step)
+    recur(0, 0)
+    for step in ORDER0[2:4]:
+        relay(step)
+    recur(1, 0)
+    for step in ORDER0[4:]:
+        relay(step)
 
     def scan(b, _):
         cols = pl.ds(pl.multiple_of(b * 128, 128), 128)
@@ -273,15 +298,11 @@
     def carry(k):
         return remote(cm, carries.at[k - 1], c_s.at[k - 1], c_r.at[k - 1], ((p + k) % 16, t))
 
-    relay(6)
-    relay(7)
-
     def carry_go(k, _):
         carry(k).start()
         return 0
 
     lax.fori_loop(1, 16, carry_go, 0)
-
     line = lax.broadcasted_iota(jnp.int32, (128, 256), 0)
     tile = jnp.where(
         line == 0, slot0,
@@ -296,90 +317,13 @@
     mix_hi[...] = high
     mix_lo[...] = (mixing - high.astype(f32)).astype(bf16)
 
-    for copy in own_w:
-        copy.wait()
-    for copy in swaps[2:5]:
-        copy.wait_recv()
-    for step in range(8):
-        i, copy = arrival(step, 1)
-        copy.wait_recv()
-        for d in range(2):
-            source = (y + 3 + 2 * d) % 4
-            remote(
-                rows.at[source, i], rows.at[source, i], f_s.at[i, d], f_r.at[i, d], partner
-            ).wait_recv()
-
-    acc[...] = jnp.zeros_like(acc)
-
-    def quarter(q, _):
-        depth = pl.ds(pl.multiple_of(q * 1024, 1024), 1024)
-        acc[...] += dot(rows[q].reshape(384, 1024), w_in[depth, :])
-        return 0
-
-    lax.fori_loop(0, 4, quarter, 0)
-    for side in range(2):
-        g = acc[:, 256 * side : 256 * side + 128]
-        u = acc[:, 256 * side + 128 : 256 * side + 256]
-        hid[:, 128 * side : 128 * side + 128] = (g / (1.0 + jnp.exp(-g)) * u).astype(bf16)
-
-    def returning(ch, step, h):
-        dz, dx = hop(step, par == o, c)
-        s = ((z + dz) % 4) * 4 + (x + dx) % 4
-        return s // 2, s, remote(
-            res.at[ch, h, s // 2], back.at[ch, p], r_s.at[ch, step, h], r_r.at[ch, p], (s, 2 * y + h)
-        )
-
-    def give(ch, _):
-        for h in range(2):
-            cols = pl.ds(pl.multiple_of(h * 2048 + ch * CW, CW), CW)
-            res[ch, h] = dot(hid[...], w_dn[:, cols]).astype(bf16).reshape(8, 48, CW)
-        for h in range(2):
-            for step in range(8):
-                i, s, copy = returning(ch, step, h)
-                if step < 7:
-                    copy.start()
-                else:
-
-                    @pl.when(jnp.logical_or(s != p, c != h))
-                    def _():
-                        copy.start()
-
-                    @pl.when(jnp.logical_and(s == p, c == h))
-                    def _():
-                        back[ch, p] = res[ch, h, i]
-
-        return 0
-
-    lax.fori_loop(0, NCH, give, 0)
-
-    def carry_in(k, _):
-        carry(k).wait_recv()
-        return 0
-
-    lax.fori_loop(1, 16, carry_in, 0)
-
-    def fold(n, state):
-        k = 15 - n
-        later = carries[k - 1]
-        return jnp.where(k <= p, later[0:4] * state + later[4:8], state)
-
-    state = lax.fori_loop(0, 15, fold, jnp.zeros((4, 128), f32))
-    for j in range(4):
-        cols = slice(128 * j, 128 * j + 128)
-        states = loc[:, cols] + acum[:, cols] * state[j : j + 1]
-        gts[0, :, cols] = (gate[:, cols] * states).astype(bf16)
-
     for copy in own_s:
         copy.wait()
     shared = dot(nx[0], w_sh[0:1024, :])
     for q in range(1, 4):
         shared = shared + dot(nx[q], w_sh[1024 * q : 1024 * q + 1024, :])
     g, u = shared[:, 0:128], shared[:, 128:256]
-    swaps[6].start()
     sh[...] = (g / (1.0 + jnp.exp(-g)) * u).astype(bf16)
-    own_o.wait()
-    swaps[1].wait_recv()
-    swaps[6].wait_recv()
     swaps[0].start()
 
     def scatter(part, recv, send_sem, recv_sem, ch):
@@ -396,11 +340,11 @@
             total.at[ch, o], other.at[ch], x_s.at[base + ch], x_r.at[base + ch], partner
         )
 
-    def settle(part, recv, total, other, send_sem, recv_sem, base):
+    def settle(part, sent, recv, total, other, send_sem, recv_sem, base):
         def one(ch, _):
-            for copy in scatter(part, recv, send_sem, recv_sem, ch):
+            for copy in scatter(sent, recv, send_sem, recv_sem, ch):
                 copy.wait_recv()
-            value = part[ch, y] + recv[ch, 0] + recv[ch, 1] + recv[ch, 2]
+            value = part[ch, y] + sum(recv[ch, k].astype(f32) for k in range(3))
             total[ch] = value.reshape(2, 32, CW)
             swap(total, other, base, ch).start()
             return 0
@@ -419,24 +363,107 @@
                 cols = pl.ds(pl.multiple_of(side * 2048 + ch * CW, CW), CW)
                 out[:, cols] = (values * factor * scale[:, cols]).astype(bf16)
 
+    swaps[0].wait_recv()
+    swaps[5].wait_recv()
+
+    def shared_part(ch, _):
+        cols = pl.ds(pl.multiple_of(ch * CW, CW), CW)
+        e_part[ch] = (dot(sh[...], s_dn[0, :, cols]) + dot(sh2[...], s_dn[1, :, cols])).reshape(4, 64, CW)
+        return 0
+
+    lax.fori_loop(0, NCH, shared_part, 0)
+
+    for copy in own_w:
+        copy.wait()
+    for copy in swaps[2:5]:
+        copy.wait_recv()
+
+    def quarter(q):
+        depth = pl.ds(pl.multiple_of(q * 1024, 1024), 1024)
+        return dot(rows[q].reshape(384, 1024), w_in[depth, :])
+
+    for step in range(FAR, 8):
+        arrival(step, 0).wait_recv()
+    acc[...] = quarter(y)
+    for step in range(8):
+        arrival(step, 1).wait_recv()
+    acc[...] += quarter((y + 2) % 4)
+    for d in range(2):
+        source = (y + 3 + 2 * d) % 4
+        for step in range(FAR, 8):
+            arrival(step, 3 - d).wait_recv()
+        for step in range(FAR):
+            remote(
+                rows.at[source, step], rows.at[source, step], f_s.at[step, d], f_r.at[step, d], partner
+            ).wait_recv()
+        acc[...] += quarter(source)
+    for side in range(2):
+        g = acc[:, 256 * side : 256 * side + 128]
+        u = acc[:, 256 * side + 128 : 256 * side + 256]
+        hid[:, 128 * side : 128 * side + 128] = (g / (1.0 + jnp.exp(-g)) * u).astype(bf16)
+
+    def returning(ch, step, h):
+        dz, dx = hop(step, par == o, par)
+        s = ((z + 4 - dz) % 4) * 4 + (x + 4 - dx) % 4
+        return step, s, remote(
+            res.at[ch, h, step], back.at[ch, p], r_s.at[ch, step, h], r_r.at[ch, p], (s, 2 * y + h)
+        )
+
+    def give(ch, _):
+        for h in range(2):
+            cols = pl.ds(pl.multiple_of(h * 2048 + ch * CW, CW), CW)
+            res[ch, h] = dot(hid[...], w_dn[:, cols]).astype(bf16).reshape(8, 48, CW)
+        for h in range(2):
+            for step in range(8):
+                i, s, copy = returning(ch, step, h)
+                if step < 7:
+                    copy.start()
+                else:
+
+                    @pl.when(jnp.logical_or(s != p, c != h))
+                    def _():
+                        copy.start()
+
+                    @pl.when(jnp.logical_and(s == p, c == h))
+                    def _():
+                        back[ch, p] = res[ch, h, i]
+
+        return 0
+
+    lax.fori_loop(0, NCH, give, 0)
+
+    def carry_in(k, _):
+        carry(k).wait_recv()
+        return 0
+
+    lax.fori_loop(1, 16, carry_in, 0)
+
+    def fold(n, state):
+        k = 15 - n
+        later = carries[k - 1]
+        return jnp.where(k <= p, later[0:4] * state + later[4:8], state)
+
+    state = lax.fori_loop(0, 15, fold, jnp.zeros((4, 128), f32))
+    for j in range(4):
+        cols = slice(128 * j, 128 * j + 128)
+        states = loc[:, cols] + acum[:, cols] * state[j : j + 1]
+        gts[0, :, cols] = (gate[:, cols] * states).astype(bf16)
+
+    swaps[6].start()
+
+    own_o.wait()
+    swaps[1].wait_recv()
+    swaps[6].wait_recv()
+
     def mixed(ch, _):
         cols = pl.ds(pl.multiple_of(ch * CW, CW), CW)
         m_part[ch] = (dot(gts[0], o_pr[0, :, cols]) + dot(gts[1], o_pr[1, :, cols])).reshape(4, 64, CW)
-        for copy in scatter(m_part, m_recv, ms_s, ms_r, ch):
+        m_send[ch] = m_part[ch].astype(bf16)
+        for copy in scatter(m_send, m_recv, ms_s, ms_r, ch):
             copy.start()
         return 0
 
     lax.fori_loop(0, NCH, mixed, 0)
-
-    swaps[0].wait_recv()
-    swaps[5].wait_recv()
-
-    def shared_part(ch, _):
-        cols = pl.ds(pl.multiple_of(ch * CW, CW), CW)
-        e_part[ch] = (dot(sh[...], s_dn[0, :, cols]) + dot(sh2[...], s_dn[1, :, cols])).reshape(4, 64, CW)
-        return 0
-
-    lax.fori_loop(0, NCH, shared_part, 0)
 
     def combine(ch, _):
         def got(e, _):
@@ -457,17 +484,15 @@
             copy.start()
         return 0
 
-    lax.fori_loop(0, NCH - 1, combine, 0)
-    settle(m_part, m_recv, m_sum, m_other, ms_s, ms_r, 0)
+    lax.fori_loop(0, NCH // 2, combine, 0)
+    settle(m_part, m_send, m_recv, m_sum, m_other, ms_s, ms_r, 0)
     finish(m_sum, m_other, mscale, out_m, 0)
-    combine(NCH - 1, 0)
-    settle(e_part, e_recv, e_sum, e_other, es_s, es_r, NCH)
-    finish(e_sum, e_other, escale, out_e, NCH)
-
-    for step in range(8):
-        for j in range(2):
-            dispatch(step, j).wait_send()
-            forward(step, j).wait_send()
+    lax.fori_loop(NCH // 2, NCH, combine, 0)
+    for step, j in order:
+        dispatch(step, j).wait_send()
+    for step in range(FAR):
+        for d in range(2):
+            forward(step, d).wait_send()
 
     def drain(ch, _):
         for step in range(8):
@@ -481,12 +506,9 @@
                     def _():
                         copy.wait_send()
 
-        for copy in scatter(m_part, m_recv, ms_s, ms_r, ch):
-            copy.wait_send()
-        for copy in scatter(e_part, e_recv, es_s, es_r, ch):
+        for copy in scatter(m_send, m_recv, ms_s, ms_r, ch):
             copy.wait_send()
         swap(m_sum, m_other, 0, ch).wait_send()
-        swap(e_sum, e_other, NCH, ch).wait_send()
         return 0
 
     lax.fori_loop(0, NCH, drain, 0)
@@ -499,6 +521,17 @@
     for copy in swaps:
         copy.wait_send()
     give_halo.wait_send()
+
+    settle(e_part, e_part, e_recv, e_sum, e_other, es_s, es_r, NCH)
+    finish(e_sum, e_other, escale, out_e, NCH)
+
+    def drain_last(ch, _):
+        for copy in scatter(e_part, e_recv, es_s, es_r, ch):
+            copy.wait_send()
+        swap(e_sum, e_other, NCH, ch).wait_send()
+        return 0
+
+    lax.fori_loop(0, NCH, drain_last, 0)
 
 
 def body(
@@ -513,16 +546,27 @@
     outs = pl.pallas_call(
         whole_kernel,
         out_shape=[jax.ShapeDtypeStruct((32, 4096), bf16)] * 2,
-        in_specs=[hbm] * 13 + [vmem] * 8,
+        in_specs=[hbm] * 21,
         out_specs=[vmem] * 2,
         scratch_shapes=[
+            pltpu.VMEM((1, 4096), f32),
+            pltpu.VMEM((4, 512), f32),
+            pltpu.VMEM((1, 512), f32),
+            pltpu.VMEM((1, 4096), f32),
+            pltpu.VMEM((1, 4096), f32),
+            pltpu.VMEM((2, 256), jnp.int32),
+            pltpu.VMEM((2, 256), f32),
+            pltpu.VMEM((1, 4096), f32),
             pltpu.VMEM((4, 256, 1024), bf16),
             pltpu.VMEM((256, 4096), bf16),
             pltpu.VMEM((2, 4096, 512), bf16),
             pltpu.VMEM((2, 2, 256, 256), bf16),
             pltpu.VMEM((2, 8, 48, 1024), bf16),
+            pltpu.VMEM((2, 8 - FAR, 48, 1024), bf16),
             pltpu.VMEM((4096, 256), bf16),
             pltpu.VMEM((256, 512), bf16),
+            pltpu.VMEM((16, 4096), bf16),
+            pltpu.VMEM((16, 512), bf16),
             pltpu.VMEM((16, 512), bf16),
             pltpu.VMEM((256, 512), f32),
             pltpu.VMEM((256, 512), f32),
@@ -546,14 +590,18 @@
         ]
         + [
             pltpu.VMEM((NCH, 4, 64, CW), f32),
+            pltpu.VMEM((NCH, 4, 64, CW), bf16),
+            pltpu.VMEM((NCH, 3, 64, CW), bf16),
+            pltpu.VMEM((NCH, 2, 32, CW), f32),
+            pltpu.VMEM((NCH, 32, CW), f32),
+            pltpu.VMEM((NCH, 4, 64, CW), f32),
             pltpu.VMEM((NCH, 3, 64, CW), f32),
             pltpu.VMEM((NCH, 2, 32, CW), f32),
             pltpu.VMEM((NCH, 32, CW), f32),
         ]
-        * 2
         + [
-            dma((8, 2)), dma((8, 2)), dma((8, 2)), dma((8, 2)), dma((15,)), dma((15,)),
-            dma((7,)), dma((7,)), dma((16,)), dma((NCH, 8, 2)), dma((NCH, 16)),
+            dma((8, 4)), dma((8, 4)), dma((8, 2)), dma((8, 2)), dma((15,)), dma((15,)),
+            dma((7,)), dma((7,)), dma((25,)), dma((NCH, 8, 2)), dma((NCH, 16)),
             dma((NCH, 3)), dma((NCH, 3)), dma((NCH, 3)), dma((NCH, 3)),
             dma((2 * NCH,)), dma((2 * NCH,)), dma((1,)), dma((1,)),
         ],
@@ -566,7 +614,19 @@
         mixer_gain[None, :], conv_taps, decay_offset[None, :], mixer_scale[None, :],
         expert_gain[None, :], route_ids.T, route_weights.T, expert_scale[None, :],
     )
-    return tuple(outs)
+
+    def hand_out(a, b, a_out, b_out):
+        a_out[...] = a[...]
+        b_out[...] = b[...]
+
+    return tuple(
+        pl.pallas_call(
+            hand_out,
+            out_shape=[jax.ShapeDtypeStruct((32, 4096), bf16)] * 2,
+            in_specs=[vmem] * 2,
+            out_specs=[vmem] * 2,
+        )(*outs)
+    )
 
 
 def solution(mesh):

time: 104 us -> 87.8 us (0.84)
  Pallas kernels: 100 us -> 87 us
  local copies, waits for them, and re-layouts: 3.34 us -> 0 us
    pallas_call x1, Pallas kernels: 100 us -> 85.1 us  [body(): pl.pallas_call(whole_kernel, out_shape=[jax.ShapeDtypeStruct((32, 4096),...]
    unnamed x2 -> x0, local copies, waits for them, and re-layouts: 3.34 us -> none
    pallas_call x0 -> x1, Pallas kernels: none -> 1.84 us  [body(): pl.pallas_call(hand_out, out_shape=[jax.ShapeDtypeStruct((32, 4096), bf16...]
where the time goes in v3:
time: 87.8 us; the launch traced here: 87.6 us
  Pallas kernels  87 us (99%)
    pallas_call x1, Pallas kernels, body(): pl.pallas_call(whole_kernel, out_shape=[jax.ShapeDtypeStruct((32, 4096),...  85.1 us
    pallas_call x1, Pallas kernels, body(): pl.pallas_call(hand_out, out_shape=[jax.ShapeDtypeStruct((32, 4096), bf16...  1.84 us

profile of v3, /device:TPU:1, one launch (start us, length us, event | category | flops | bytes accessed | tf_op | source)
XLA Modules:
  0.0 87.6 jit_solution(15002745879853794232)
XLA Ops:
  0.6 85.1 %shard_map.212 = (bf16[32,4096]{1,0:T(8,128)(2,1)}, bf16[32,4096]{1,0:T(8,128)(2,1)}) custom-call(bf16[256,4096]{1,0:T(8,128)(2,1)} %m_rows.1, bf16[4096,512]{1,0:T(8,128)(2,1)} %g_proj.1, bf16[4096,512]{1,0:T(8,128)(2,1)} %i_proj.1, bf16[2,256,256]{2,1,0:T(8,128)(2,1)} %i_gates.1, bf16[2,256,256]{2,1,0:T(8,128)(2,1)} %d_gates.1, bf16[512,4096]{1,0:T(8,128)(2,1)} %op.1, ...), custom_call_target="tpu_custom_call" | custom-call | tf_op jit(solution)/shard_map/pallas_call | solution.py:546
  85.8 1.8 %shard_map.213 = (bf16[32,4096]{1,0:T(8,128)(2,1)}, bf16[32,4096]{1,0:T(8,128)(2,1)}) custom-call(bf16[32,4096]{1,0:T(8,128)(2,1)} %get-tuple-element.4.a, bf16[32,4096]{1,0:T(8,128)(2,1)} %get-tuple-element.5.b), custom_call_target="tpu_custom_call" | custom-call | tf_op jit(solution)/shard_map/pallas_call | solution.py:623

commit v4 on v3

--- a/solution.py
+++ b/solution.py
@@ -12,7 +12,7 @@
 MESH = pl.DeviceIdType.MESH
 NCH = 8
 FAR = 6
-ORDER0 = (5, 4, 3, 2, 1, 0)
+LEAD = 2
 CW = 2048 // NCH
 FAR_EVEN = ((2, 2), (1, 2), (3, 2), (2, 0), (0, 2), (1, 0), (3, 0), (0, 0))
 FAR_ODD = ((2, 1), (2, 3), (1, 1), (3, 3), (1, 3), (3, 1), (0, 1), (0, 3))
@@ -53,7 +53,7 @@
     m_gain, taps, offset, mscale, x_gain, ids, weights, escale,
     nx, nm, proj, bgates, send_x, send_n, w_sh, br, tail, edge, halo, gate, acum, loc, cm, sh, mix_hi, mix_lo,
     rows, w_in, w_dn, s_dn, o_pr, sh2, gts, carries, acc, hid, res, back,
-    m_part, m_send, m_recv, m_sum, m_other, e_part, e_recv, e_sum, e_other,
+    m_part, m_send, m_recv, m_sum, m_other, e_part, e_recv, e_sum,
     d_s, d_r, f_s, f_r, c_s, c_r, p_s, p_r, l_s, r_s, r_r, ms_s, ms_r, es_s, es_r, x_s, x_r, h_s, h_r,
 ):
     f32, bf16 = jnp.float32, jnp.bfloat16
@@ -71,6 +71,33 @@
     def dot(a, b):
         return jnp.dot(a, b, preferred_element_type=f32)
 
+    def wide(at):
+        return pl.ds(pl.multiple_of(at * 2048, 2048), 2048)
+
+    def local(src, dst, n):
+        return pltpu.make_async_copy(src, dst, l_s.at[n])
+
+    early = [local(m_rows.at[240:256], tail, 1), local(i_proj, proj.at[1], 2)]
+    first = [local(x_rows.at[:, 1024 * q : 1024 * q + 1024], nx.at[q], 0) for q in range(4)]
+    second = [local(m_rows, nm, 3), local(g_proj, proj.at[0], 4)]
+    gates_in = [local(i_gates, bgates.at[0], 5), local(d_gates, bgates.at[1], 6)]
+    own_w = [
+        local(eg, w_in.at[:, 0:128], 7),
+        local(eu, w_in.at[:, 128:256], 8),
+        local(ed, w_dn.at[0:128], 9),
+    ]
+    own_o = local(op.at[:, wide(c)], o_pr.at[0], 10)
+    own_s = [
+        local(sd.at[:, wide(c)], s_dn.at[0], 11),
+        local(sg, w_sh.at[:, 0:128], 12),
+        local(su, w_sh.at[:, 128:256], 13),
+    ]
+    small = [local(ids_h, ids, 14), local(weights_h, weights, 15), local(x_gain_h, x_gain, 16)]
+    small += [local(m_gain_h, m_gain, 17), local(taps_h, taps, 18), local(offset_h, offset, 19)]
+    small += [local(mscale_h, mscale, 20), local(escale_h, escale, 21)]
+    for copy in small[:1] + first + small[1:]:
+        copy.start()
+
     barrier = pltpu.get_barrier_semaphore()
 
     def greet(k, _):
@@ -86,33 +113,13 @@
             barrier, inc=1, device_id=(p, 2 * ((y + k) % 4) + c), device_id_type=MESH
         )
 
-    def wide(at):
-        return pl.ds(pl.multiple_of(at * 2048, 2048), 2048)
-
-    def local(src, dst, n):
-        return pltpu.make_async_copy(src, dst, l_s.at[n])
-
-    early = [local(m_rows.at[240:256], tail, 16), local(i_proj, proj.at[1], 5)]
-    first = [local(x_rows.at[:, 1024 * q : 1024 * q + 1024], nx.at[q], q) for q in range(4)]
-    second = [local(m_rows, nm, 4), local(g_proj, proj.at[0], 6)]
-    gates_in = [local(i_gates, bgates.at[0], 7), local(d_gates, bgates.at[1], 8)]
-    own_w = [
-        local(eg, w_in.at[:, 0:128], 9),
-        local(eu, w_in.at[:, 128:256], 10),
-        local(ed, w_dn.at[0:128], 11),
-    ]
-    own_o = local(op.at[:, wide(c)], o_pr.at[0], 12)
-    own_s = [
-        local(sd.at[:, wide(c)], s_dn.at[0], 13),
-        local(sg, w_sh.at[:, 0:128], 14),
-        local(su, w_sh.at[:, 128:256], 15),
-    ]
-    small = [local(ids_h, ids, 17), local(weights_h, weights, 18), local(x_gain_h, x_gain, 19)]
-    small += [local(m_gain_h, m_gain, 20), local(taps_h, taps, 21), local(offset_h, offset, 22)]
-    small += [local(mscale_h, mscale, 23), local(escale_h, escale, 24)]
-    for copy in small[:1] + first + small[1:]:
-        copy.start()
     small[0].wait()
+
+    def await_recv(group, sem):
+        remote(group, group, h_s.at[0], sem, partner).wait_recv()
+
+    def await_send(group, sem):
+        remote(group, group, sem, h_r.at[0], partner).wait_send()
 
     id0, id1 = ids[0:1, :], ids[1:2, :]
     expert = lax.broadcasted_iota(jnp.int32, (16, 256), 0)
@@ -133,7 +140,8 @@
 
     chosen = jnp.concatenate([picked(i) for i in range(8)], axis=0)
 
-    for copy in first + small[1:]:
+    local(nx, nx, 0).wait()
+    for copy in small[1:]:
         copy.wait()
     for copy in early + second + gates_in:
         copy.start()
@@ -142,32 +150,10 @@
         at = pl.ds(pl.multiple_of(r * 32, 32), 32)
         parts = [nx[q, at, :].astype(f32) for q in range(4)]
         square = sum(jnp.sum(v * v, axis=1, keepdims=True) for v in parts)
-        factor = lax.rsqrt(square / 4096.0 + eps)
+        scale = lax.rsqrt(square / 4096.0 + eps)
         for q in range(4):
-            nx[q, at, :] = (parts[q] * factor * x_gain[:, 1024 * q : 1024 * q + 1024]).astype(bf16)
-        return 0
-
-    lax.fori_loop(0, 8, norm_x, 0)
-    for j in range(2):
-        send_x[j] = dot(chosen, nx[(y + 2 * j) % 4]).astype(bf16).reshape(8, 48, 1024)
-    near = []
-    for step in range(FAR, 8):
-        dz, dx = hop(step, par == c, c)
-        near.append(((((z + dz) % 4) * 4 + (x + dx) % 4) // 2))
-    near_chosen = jnp.concatenate([picked(i) for i in near], axis=0)
-    for j in range(2):
-        send_n[j] = dot(near_chosen, nx[(y + 1 + 2 * j) % 4]).astype(bf16).reshape(8 - FAR, 48, 1024)
-
-    for copy in early:
-        copy.wait()
-    v = tail[...].astype(f32)
-    factor = lax.rsqrt(jnp.sum(v * v, axis=1, keepdims=True) / 4096.0 + eps)
-    last_rows = (v * factor * m_gain[...]).astype(bf16)
-    edge[...] = dot(last_rows, proj[1]).astype(bf16)
-
-    pl.semaphore_wait(barrier, 34)
-    give_halo = remote(edge, halo, h_s.at[0], h_r.at[0], ((p + 1) % 16, t))
-    give_halo.start()
+            nx[q, at, :] = (parts[q] * scale * x_gain[:, 1024 * q : 1024 * q + 1024]).astype(bf16)
+        return 0
 
     def dispatch(step, j):
         dz, dx = hop(step, par == c, c)
@@ -175,20 +161,52 @@
         source = send_x.at[j, e // 2] if j < 2 else send_n.at[j - 2, step - FAR]
         shift = (0, 2, 1, 3)[j]
         return remote(
-            source, rows.at[(y + shift) % 4, step], d_s.at[step, j], d_r.at[step, j],
+            source, rows.at[(y + shift) % 4, step], d_s.at[j // 2], d_r.at[landing(step, j)],
             (e, 2 * y + 1 - par),
         )
 
-    def arrival(step, j):
+    def landing(step, j):
+        if j == 0:
+            return min(step, FAR)
+        return FAR + (1 + step // 4 if j == 1 else 1 + j)
+
+    def group(low, high, j):
         shift = (0, 2, 1, 3)[j]
-        return remote(
-            send_x.at[0, 0], rows.at[(y + shift) % 4, step], d_s.at[step, j], d_r.at[step, j], partner
-        )
-
-    order = [(step, 0) for step in ORDER0] + [(step, 1) for step in range(8)]
-    order += [(step, j) for step in range(FAR, 8) for j in (0, 2, 3)]
-    for step, j in order:
-        dispatch(step, j).start()
+        await_recv(rows.at[(y + shift) % 4, low:high], d_r.at[landing(low, j)])
+
+    def gather(j):
+        send_x[j] = dot(chosen, nx[(y + 2 * j) % 4]).astype(bf16).reshape(8, 48, 1024)
+
+    lax.fori_loop(0, 8, norm_x, 0)
+    gather(0)
+    pl.semaphore_wait(barrier, 34)
+    for step in range(4):
+        dispatch(step, 0).start()
+    gather(1)
+    for step in range(4):
+        dispatch(step, 1).start()
+
+    for copy in early:
+        copy.wait()
+    v = tail[...].astype(f32)
+    tail_factor = lax.rsqrt(jnp.sum(v * v, axis=1, keepdims=True) / 4096.0 + eps)
+    edge[...] = dot((v * tail_factor * m_gain[...]).astype(bf16), proj[1]).astype(bf16)
+    give_halo = remote(edge, halo, h_s.at[0], h_r.at[0], ((p + 1) % 16, t))
+    give_halo.start()
+    for j in range(2):
+        for step in range(4, FAR):
+            dispatch(step, j).start()
+
+    near = []
+    for step in range(FAR, 8):
+        dz, dx = hop(step, par == c, c)
+        near.append((((z + dz) % 4) * 4 + (x + dx) % 4) // 2)
+    near_chosen = jnp.concatenate([picked(i) for i in near], axis=0)
+    for j in range(2):
+        send_n[j] = dot(near_chosen, nx[(y + 1 + 2 * j) % 4]).astype(bf16).reshape(8 - FAR, 48, 1024)
+    for j in range(4):
+        for step in range(FAR, 8):
+            dispatch(step, j).start()
 
     swaps = [
         remote(sh, sh2, p_s.at[0], p_r.at[0], partner),
@@ -204,12 +222,12 @@
 
     def forward(i, d):
         return remote(
-            rows.at[y, i], rows.at[y, i], f_s.at[i, d], f_r.at[i, d],
+            rows.at[y, i], rows.at[y, i], f_s.at[0], f_r.at[i // 4, d],
             (p, 2 * ((y + 1 + 2 * d) % 4) + c),
         )
 
     def relay(step):
-        arrival(step, 0).wait_recv()
+        group(step, step + 1, 0)
         forward(step, 0).start()
         forward(step, 1).start()
 
@@ -218,8 +236,8 @@
     def norm_m(r, _):
         at = pl.ds(pl.multiple_of(r * 32, 32), 32)
         v = nm[at, :].astype(f32)
-        factor = lax.rsqrt(jnp.sum(v * v, axis=1, keepdims=True) / 4096.0 + eps)
-        nm[at, :] = (v * factor * m_gain[...]).astype(bf16)
+        scale = lax.rsqrt(jnp.sum(v * v, axis=1, keepdims=True) / 4096.0 + eps)
+        nm[at, :] = (v * scale * m_gain[...]).astype(bf16)
         return 0
 
     lax.fori_loop(0, 8, norm_m, 0)
@@ -238,7 +256,12 @@
         gate[:, cols] = 0.5 * v * (1.0 + jnp.tanh(0.7978845608028654 * (v + 0.044715 * (v * v * v))))
         return 0
 
-    lax.fori_loop(0, 2, gates, 0)
+    relay(0)
+    relay(1)
+    gates(0, 0)
+    relay(2)
+    gates(1, 0)
+    relay(3)
     for copy in gates_in:
         copy.wait()
     give_halo.wait_recv()
@@ -266,14 +289,10 @@
         acum[:, cols] = jnp.exp(log_decay)
         return 0
 
-    for step in ORDER0[:2]:
-        relay(step)
     recur(0, 0)
-    for step in ORDER0[2:4]:
-        relay(step)
+    relay(4)
     recur(1, 0)
-    for step in ORDER0[4:]:
-        relay(step)
+    relay(5)
 
     def scan(b, _):
         cols = pl.ds(pl.multiple_of(b * 128, 128), 128)
@@ -296,7 +315,7 @@
     lax.fori_loop(0, 4, scan, 0)
 
     def carry(k):
-        return remote(cm, carries.at[k - 1], c_s.at[k - 1], c_r.at[k - 1], ((p + k) % 16, t))
+        return remote(cm, carries.at[k - 1], c_s.at[0], c_r.at[0], ((p + k) % 16, t))
 
     def carry_go(k, _):
         carry(k).start()
@@ -329,21 +348,21 @@
     def scatter(part, recv, send_sem, recv_sem, ch):
         return [
             remote(
-                part.at[ch, (y + k) % 4], recv.at[ch, k - 1], send_sem.at[ch, k - 1],
-                recv_sem.at[ch, k - 1], (p, 2 * ((y + k) % 4) + c),
+                part.at[ch, (y + k) % 4], recv.at[ch, k - 1], send_sem.at[0],
+                recv_sem.at[0], (p, 2 * ((y + k) % 4) + c),
             )
             for k in range(1, 4)
         ]
 
     def swap(total, other, base, ch):
         return remote(
-            total.at[ch, o], other.at[ch], x_s.at[base + ch], x_r.at[base + ch], partner
+            total.at[ch, o], other.at[ch], x_s.at[0], x_r.at[0], partner
         )
 
     def settle(part, sent, recv, total, other, send_sem, recv_sem, base):
+        await_recv(recv, recv_sem.at[0])
+
         def one(ch, _):
-            for copy in scatter(sent, recv, send_sem, recv_sem, ch):
-                copy.wait_recv()
             value = part[ch, y] + sum(recv[ch, k].astype(f32) for k in range(3))
             total[ch] = value.reshape(2, 32, CW)
             swap(total, other, base, ch).start()
@@ -353,90 +372,85 @@
 
     def finish(total, other, scale, out, base):
         square = jnp.zeros((32, 1), f32)
+        await_recv(other, x_r.at[0])
         for ch in range(NCH):
-            swap(total, other, base, ch).wait_recv()
             mine, theirs = total[ch, c], other[ch]
             square += jnp.sum(mine * mine + theirs * theirs, axis=1, keepdims=True)
-        factor = lax.rsqrt(square / 4096.0 + eps)
+        level = lax.rsqrt(square / 4096.0 + eps)
         for ch in range(NCH):
             for values, side in ((total[ch, c], c), (other[ch], o)):
                 cols = pl.ds(pl.multiple_of(side * 2048 + ch * CW, CW), CW)
-                out[:, cols] = (values * factor * scale[:, cols]).astype(bf16)
-
-    swaps[0].wait_recv()
-    swaps[5].wait_recv()
-
-    def shared_part(ch, _):
-        cols = pl.ds(pl.multiple_of(ch * CW, CW), CW)
-        e_part[ch] = (dot(sh[...], s_dn[0, :, cols]) + dot(sh2[...], s_dn[1, :, cols])).reshape(4, 64, CW)
-        return 0
-
-    lax.fori_loop(0, NCH, shared_part, 0)
+                out[:, cols] = (values * level * scale[:, cols]).astype(bf16)
 
     for copy in own_w:
         copy.wait()
     for copy in swaps[2:5]:
         copy.wait_recv()
 
-    def quarter(q):
-        depth = pl.ds(pl.multiple_of(q * 1024, 1024), 1024)
-        return dot(rows[q].reshape(384, 1024), w_in[depth, :])
-
-    for step in range(FAR, 8):
-        arrival(step, 0).wait_recv()
-    acc[...] = quarter(y)
-    for step in range(8):
-        arrival(step, 1).wait_recv()
-    acc[...] += quarter((y + 2) % 4)
-    for d in range(2):
-        source = (y + 3 + 2 * d) % 4
-        for step in range(FAR, 8):
-            arrival(step, 3 - d).wait_recv()
-        for step in range(FAR):
-            remote(
-                rows.at[source, step], rows.at[source, step], f_s.at[step, d], f_r.at[step, d], partner
-            ).wait_recv()
-        acc[...] += quarter(source)
-    for side in range(2):
-        g = acc[:, 256 * side : 256 * side + 128]
-        u = acc[:, 256 * side + 128 : 256 * side + 256]
-        hid[:, 128 * side : 128 * side + 128] = (g / (1.0 + jnp.exp(-g)) * u).astype(bf16)
+    def hidden(half_of):
+        at = slice(192 * half_of, 192 * half_of + 192)
+
+        def quarter(q):
+            depth = pl.ds(pl.multiple_of(q * 1024, 1024), 1024)
+            block = rows[q, 4 * half_of : 4 * half_of + 4].reshape(192, 1024)
+            return dot(block, w_in[depth, :])
+
+        if half_of == 1:
+            group(FAR, 8, 0)
+        acc[at] = quarter(y)
+        group(4 * half_of, 4 * half_of + 4, 1)
+        acc[at] += quarter((y + 2) % 4)
+        for d in range(2):
+            source = (y + 3 + 2 * d) % 4
+            await_recv(rows.at[source, 4 * half_of : min(FAR, 4 * half_of + 4)], f_r.at[half_of, d])
+            if half_of == 1:
+                group(FAR, 8, 3 - d)
+            acc[at] += quarter(source)
+        for side in range(2):
+            g = acc[at, 256 * side : 256 * side + 128]
+            u = acc[at, 256 * side + 128 : 256 * side + 256]
+            hid[at, 128 * side : 128 * side + 128] = (g / (1.0 + jnp.exp(-g)) * u).astype(bf16)
 
     def returning(ch, step, h):
         dz, dx = hop(step, par == o, par)
         s = ((z + 4 - dz) % 4) * 4 + (x + 4 - dx) % 4
-        return step, s, remote(
-            res.at[ch, h, step], back.at[ch, p], r_s.at[ch, step, h], r_r.at[ch, p], (s, 2 * y + h)
+        return s, remote(
+            res.at[ch, h, step], back.at[ch, p], r_s.at[ch], r_r.at[ch], (s, 2 * y + h)
         )
 
-    def give(ch, _):
-        for h in range(2):
-            cols = pl.ds(pl.multiple_of(h * 2048 + ch * CW, CW), CW)
-            res[ch, h] = dot(hid[...], w_dn[:, cols]).astype(bf16).reshape(8, 48, CW)
-        for h in range(2):
-            for step in range(8):
-                i, s, copy = returning(ch, step, h)
-                if step < 7:
-                    copy.start()
-                else:
-
-                    @pl.when(jnp.logical_or(s != p, c != h))
-                    def _():
+    def give(low, high):
+        def one(ch, _):
+            for h in range(2):
+                cols = pl.ds(pl.multiple_of(h * 2048 + ch * CW, CW), CW)
+                res[ch, h, low:high] = (
+                    dot(hid[48 * low : 48 * high], w_dn[:, cols]).astype(bf16).reshape(high - low, 48, CW)
+                )
+            for h in range(2):
+                for step in range(low, high):
+                    s, copy = returning(ch, step, h)
+                    if step < 7:
                         copy.start()
-
-                    @pl.when(jnp.logical_and(s == p, c == h))
-                    def _():
-                        back[ch, p] = res[ch, h, i]
-
-        return 0
-
-    lax.fori_loop(0, NCH, give, 0)
-
-    def carry_in(k, _):
-        carry(k).wait_recv()
-        return 0
-
-    lax.fori_loop(1, 16, carry_in, 0)
+                    else:
+
+                        @pl.when(jnp.logical_or(s != p, c != h))
+                        def _():
+                            copy.start()
+
+                        @pl.when(jnp.logical_and(s == p, c == h))
+                        def _():
+                            back[ch, p] = res[ch, h, step]
+
+            return 0
+
+        return one
+
+    hidden(0)
+    lax.fori_loop(0, LEAD, give(0, 4), 0)
+    hidden(1)
+    lax.fori_loop(0, LEAD, give(4, 8), 0)
+    lax.fori_loop(LEAD, NCH, give(0, 8), 0)
+
+    await_recv(carries, c_r.at[0])
 
     def fold(n, state):
         k = 15 - n
@@ -465,22 +479,40 @@
 
     lax.fori_loop(0, NCH, mixed, 0)
 
+    swaps[0].wait_recv()
+    swaps[5].wait_recv()
+
+    def shared_part(ch, _):
+        cols = pl.ds(pl.multiple_of(ch * CW, CW), CW)
+        e_part[ch] = (dot(sh[...], s_dn[0, :, cols]) + dot(sh2[...], s_dn[1, :, cols])).reshape(4, 2, 32, CW)
+        return 0
+
+    lax.fori_loop(0, NCH, shared_part, 0)
+
+    def final(ch):
+        return [
+            remote(
+                e_part.at[ch, (y + k) % 4, w], e_recv.at[ch, 2 * (k - 1) + c], es_s.at[0],
+                es_r.at[ch], (p, 2 * ((y + k) % 4) + w),
+            )
+            for k in range(1, 4)
+            for w in range(2)
+        ] + [remote(e_part.at[ch, y, o], e_recv.at[ch, 6], es_s.at[1], es_r.at[ch], partner)]
+
     def combine(ch, _):
-        def got(e, _):
-            @pl.when(jnp.logical_or(e != p, c != 1 - par))
-            def _():
-                remote(
-                    res.at[ch, 0, 0], back.at[ch, e], r_s.at[ch, 0, 0], r_r.at[ch, e], partner
-                ).wait_recv()
-
-            return 0
-
-        lax.fori_loop(0, 16, got, 0)
+        @pl.when(par == o)
+        def _():
+            await_recv(back.at[ch, 0:15], r_r.at[ch])
+
+        @pl.when(par != o)
+        def _():
+            await_recv(back.at[ch], r_r.at[ch])
+
         returned = back[ch].reshape(768, CW)
         e_part[ch] = e_part[ch] + (
             dot(mix_hi[...], returned) + dot(mix_lo[...], returned)
-        ).reshape(4, 64, CW)
-        for copy in scatter(e_part, e_recv, es_s, es_r, ch):
+        ).reshape(4, 2, 32, CW)
+        for copy in final(ch):
             copy.start()
         return 0
 
@@ -488,50 +520,44 @@
     settle(m_part, m_send, m_recv, m_sum, m_other, ms_s, ms_r, 0)
     finish(m_sum, m_other, mscale, out_m, 0)
     lax.fori_loop(NCH // 2, NCH, combine, 0)
-    for step, j in order:
-        dispatch(step, j).wait_send()
-    for step in range(FAR):
-        for d in range(2):
-            forward(step, d).wait_send()
-
-    def drain(ch, _):
-        for step in range(8):
-            for h in range(2):
-                i, s, copy = returning(ch, step, h)
-                if step < 7:
-                    copy.wait_send()
-                else:
-
-                    @pl.when(jnp.logical_or(s != p, c != h))
-                    def _():
-                        copy.wait_send()
-
-        for copy in scatter(m_send, m_recv, ms_s, ms_r, ch):
-            copy.wait_send()
-        swap(m_sum, m_other, 0, ch).wait_send()
-        return 0
-
-    lax.fori_loop(0, NCH, drain, 0)
-
-    def carry_out(k, _):
-        carry(k).wait_send()
-        return 0
-
-    lax.fori_loop(1, 16, carry_out, 0)
+    await_send(send_x, d_s.at[0])
+    await_send(send_n, d_s.at[1])
+    await_send(rows.at[0:2, 0:FAR], f_s.at[0])
+    await_send(carries, c_s.at[0])
+
+    @pl.when(par == o)
+    def _():
+        for ch in range(NCH):
+            await_send(back.at[ch, 0:15], r_s.at[ch])
+
+    @pl.when(par != o)
+    def _():
+        for ch in range(NCH):
+            await_send(back.at[ch], r_s.at[ch])
+
+    await_send(m_recv, ms_s.at[0])
+    await_send(m_other, x_s.at[0])
     for copy in swaps:
         copy.wait_send()
     give_halo.wait_send()
 
-    settle(e_part, e_part, e_recv, e_sum, e_other, es_s, es_r, NCH)
-    finish(e_sum, e_other, escale, out_e, NCH)
-
-    def drain_last(ch, _):
-        for copy in scatter(e_part, e_recv, es_s, es_r, ch):
-            copy.wait_send()
-        swap(e_sum, e_other, NCH, ch).wait_send()
-        return 0
-
-    lax.fori_loop(0, NCH, drain_last, 0)
+    def settle_last(ch, square):
+        await_recv(e_recv.at[ch, 0:7], es_r.at[ch])
+        mine = e_part[ch, y, c] + e_recv[ch, c] + e_recv[ch, 2 + c] + e_recv[ch, 4 + c]
+        theirs = e_recv[ch, 6] + e_recv[ch, o] + e_recv[ch, 2 + o] + e_recv[ch, 4 + o]
+        e_sum[ch, c] = mine
+        e_sum[ch, o] = theirs
+        return square + jnp.sum(mine * mine + theirs * theirs, axis=1, keepdims=True)
+
+    square = lax.fori_loop(0, NCH, settle_last, jnp.zeros((32, 1), f32))
+    level = lax.rsqrt(square / 4096.0 + eps)
+    for ch in range(NCH):
+        for w in range(2):
+            cols = slice(w * 2048 + ch * CW, w * 2048 + ch * CW + CW)
+            out_e[:, cols] = (e_sum[ch, w] * level * escale[:, cols]).astype(bf16)
+
+    await_send(e_part.at[:, 1:4], es_s.at[0])
+    await_send(e_part.at[:, 0, 0], es_s.at[1])
 
 
 def body(
@@ -594,16 +620,14 @@
             pltpu.VMEM((NCH, 3, 64, CW), bf16),
             pltpu.VMEM((NCH, 2, 32, CW), f32),
             pltpu.VMEM((NCH, 32, CW), f32),
-            pltpu.VMEM((NCH, 4, 64, CW), f32),
-            pltpu.VMEM((NCH, 3, 64, CW), f32),
+            pltpu.VMEM((NCH, 4, 2, 32, CW), f32),
+            pltpu.VMEM((NCH, 7, 32, CW), f32),
             pltpu.VMEM((NCH, 2, 32, CW), f32),
-            pltpu.VMEM((NCH, 32, CW), f32),
         ]
         + [
-            dma((8, 4)), dma((8, 4)), dma((8, 2)), dma((8, 2)), dma((15,)), dma((15,)),
-            dma((7,)), dma((7,)), dma((25,)), dma((NCH, 8, 2)), dma((NCH, 16)),
-            dma((NCH, 3)), dma((NCH, 3)), dma((NCH, 3)), dma((NCH, 3)),
-            dma((2 * NCH,)), dma((2 * NCH,)), dma((1,)), dma((1,)),
+            dma((2,)), dma((FAR + 5,)), dma((1,)), dma((2, 2)), dma((1,)), dma((1,)),
+            dma((7,)), dma((7,)), dma((22,)), dma((NCH,)), dma((NCH,)),
+            dma((1,)), dma((1,)), dma((2,)), dma((NCH,)), dma((1,)), dma((1,)), dma((1,)), dma((1,)),
         ],
         compiler_params=pltpu.CompilerParams(
             collective_id=0, has_side_effects=True, vmem_limit_bytes=67043328

time: 87.8 us -> 79.9 us (0.910)
  Pallas kernels: 87 us -> 79.1 us
    pallas_call x1, Pallas kernels: 85.1 us -> 77.3 us  [body(): pl.pallas_call(whole_kernel, out_shape=[jax.ShapeDtypeStruct((32, 4096),...]
where the time goes in v4:
time: 79.9 us; the launch traced here: 79.8 us
  Pallas kernels  79.1 us (99%)
    pallas_call x1, Pallas kernels, body(): pl.pallas_call(whole_kernel, out_shape=[jax.ShapeDtypeStruct((32, 4096),...  77.3 us
    pallas_call x1, Pallas kernels, body(): pl.pallas_call(hand_out, out_shape=[jax.ShapeDtypeStruct((32, 4096), bf16...  1.84 us

profile of v4, /device:TPU:1, one launch (start us, length us, event | category | flops | bytes accessed | tf_op | source)
XLA Modules:
  0.0 79.8 jit_solution(2436813539001241872)
XLA Ops:
  0.6 77.3 %shard_map.212 = (bf16[32,4096]{1,0:T(8,128)(2,1)}, bf16[32,4096]{1,0:T(8,128)(2,1)}) custom-call(bf16[256,4096]{1,0:T(8,128)(2,1)} %m_rows.1, bf16[4096,512]{1,0:T(8,128)(2,1)} %g_proj.1, bf16[4096,512]{1,0:T(8,128)(2,1)} %i_proj.1, bf16[2,256,256]{2,1,0:T(8,128)(2,1)} %i_gates.1, bf16[2,256,256]{2,1,0:T(8,128)(2,1)} %d_gates.1, bf16[512,4096]{1,0:T(8,128)(2,1)} %op.1, ...), custom_call_target="tpu_custom_call" | custom-call | tf_op jit(solution)/shard_map/pallas_call | solution.py:572
  77.9 1.8 %shard_map.213 = (bf16[32,4096]{1,0:T(8,128)(2,1)}, bf16[32,4096]{1,0:T(8,128)(2,1)}) custom-call(bf16[32,4096]{1,0:T(8,128)(2,1)} %get-tuple-element.4.a, bf16[32,4096]{1,0:T(8,128)(2,1)} %get-tuple-element.5.b), custom_call_target="tpu_custom_call" | custom-call | tf_op jit(solution)/shard_map/pallas_call | solution.py:647

commit v5 on v4

--- a/solution.py
+++ b/solution.py
@@ -10,9 +10,9 @@
 
 
 MESH = pl.DeviceIdType.MESH
-NCH = 8
-FAR = 6
-LEAD = 2
+NCH = 4
+FAR = 7
+LEAD = 1
 CW = 2048 // NCH
 FAR_EVEN = ((2, 2), (1, 2), (3, 2), (2, 0), (0, 2), (1, 0), (3, 0), (0, 0))
 FAR_ODD = ((2, 1), (2, 3), (1, 1), (3, 3), (1, 3), (3, 1), (0, 1), (0, 3))
@@ -78,7 +78,13 @@
         return pltpu.make_async_copy(src, dst, l_s.at[n])
 
     early = [local(m_rows.at[240:256], tail, 1), local(i_proj, proj.at[1], 2)]
-    first = [local(x_rows.at[:, 1024 * q : 1024 * q + 1024], nx.at[q], 0) for q in range(4)]
+    first = [
+        local(
+            x_rows.at[r : r + 128, 1024 * q : 1024 * q + 1024], nx.at[q, r : r + 128], 22 if r else 0
+        )
+        for r in (0, 128)
+        for q in range(4)
+    ]
     second = [local(m_rows, nm, 3), local(g_proj, proj.at[0], 4)]
     gates_in = [local(i_gates, bgates.at[0], 5), local(d_gates, bgates.at[1], 6)]
     own_w = [
@@ -140,11 +146,8 @@
 
     chosen = jnp.concatenate([picked(i) for i in range(8)], axis=0)
 
-    local(nx, nx, 0).wait()
     for copy in small[1:]:
         copy.wait()
-    for copy in early + second + gates_in:
-        copy.start()
 
     def norm_x(r, _):
         at = pl.ds(pl.multiple_of(r * 32, 32), 32)
@@ -177,7 +180,12 @@
     def gather(j):
         send_x[j] = dot(chosen, nx[(y + 2 * j) % 4]).astype(bf16).reshape(8, 48, 1024)
 
-    lax.fori_loop(0, 8, norm_x, 0)
+    local(nx.at[:, 0:128], nx.at[:, 0:128], 0).wait()
+    lax.fori_loop(0, 4, norm_x, 0)
+    local(nx.at[:, 128:256], nx.at[:, 128:256], 22).wait()
+    for copy in early + second + gates_in:
+        copy.start()
+    lax.fori_loop(4, 8, norm_x, 0)
     gather(0)
     pl.semaphore_wait(barrier, 34)
     for step in range(4):
@@ -293,6 +301,7 @@
     relay(4)
     recur(1, 0)
     relay(5)
+    relay(6)
 
     def scan(b, _):
         cols = pl.ds(pl.multiple_of(b * 128, 128), 128)
@@ -626,7 +635,7 @@
         ]
         + [
             dma((2,)), dma((FAR + 5,)), dma((1,)), dma((2, 2)), dma((1,)), dma((1,)),
-            dma((7,)), dma((7,)), dma((22,)), dma((NCH,)), dma((NCH,)),
+            dma((7,)), dma((7,)), dma((23,)), dma((NCH,)), dma((NCH,)),
             dma((1,)), dma((1,)), dma((2,)), dma((NCH,)), dma((1,)), dma((1,)), dma((1,)), dma((1,)),
         ],
         compiler_params=pltpu.CompilerParams(

time: 79.9 us -> 79.4 us (level)
  no operation moved by 1% of the time
where the time goes in v5:
time: 79.4 us; the launch traced here: 79.2 us
  Pallas kernels  78.6 us (99%)
    pallas_call x1, Pallas kernels, body(): pl.pallas_call(whole_kernel, out_shape=[jax.ShapeDtypeStruct((32, 4096),...  76.7 us
    pallas_call x1, Pallas kernels, body(): pl.pallas_call(hand_out, out_shape=[jax.ShapeDtypeStruct((32, 4096), bf16...  1.84 us

profile of v5, /device:TPU:1, one launch (start us, length us, event | category | flops | bytes accessed | tf_op | source)
XLA Modules:
  0.0 79.2 jit_solution(6037273461172496789)
XLA Ops:
  0.6 76.7 %shard_map.212 = (bf16[32,4096]{1,0:T(8,128)(2,1)}, bf16[32,4096]{1,0:T(8,128)(2,1)}) custom-call(bf16[256,4096]{1,0:T(8,128)(2,1)} %m_rows.1, bf16[4096,512]{1,0:T(8,128)(2,1)} %g_proj.1, bf16[4096,512]{1,0:T(8,128)(2,1)} %i_proj.1, bf16[2,256,256]{2,1,0:T(8,128)(2,1)} %i_gates.1, bf16[2,256,256]{2,1,0:T(8,128)(2,1)} %d_gates.1, bf16[512,4096]{1,0:T(8,128)(2,1)} %op.1, ...), custom_call_target="tpu_custom_call" | custom-call | tf_op jit(solution)/shard_map/pallas_call | solution.py:581
  77.4 1.8 %shard_map.213 = (bf16[32,4096]{1,0:T(8,128)(2,1)}, bf16[32,4096]{1,0:T(8,128)(2,1)}) custom-call(bf16[32,4096]{1,0:T(8,128)(2,1)} %get-tuple-element.4.a, bf16[32,4096]{1,0:T(8,128)(2,1)} %get-tuple-element.5.b), custom_call_target="tpu_custom_call" | custom-call | tf_op jit(solution)/shard_map/pallas_call | solution.py:656

commit v6 on v5

--- a/solution.py
+++ b/solution.py
@@ -106,14 +106,11 @@
 
     barrier = pltpu.get_barrier_semaphore()
 
-    def greet(k, _):
-        other = (p * 2 + c + k) % 32
+    for k in range(1, 32):
+        other = lax.rem(p * 2 + c + k, 32)
         pl.semaphore_signal(
-            barrier, inc=1, device_id=(other // 2, 2 * y + other % 2), device_id_type=MESH
+            barrier, inc=1, device_id=(lax.div(other, 2), 2 * y + lax.rem(other, 2)), device_id_type=MESH
         )
-        return 0
-
-    lax.fori_loop(1, 32, greet, 0)
     for k in range(1, 4):
         pl.semaphore_signal(
             barrier, inc=1, device_id=(p, 2 * ((y + k) % 4) + c), device_id_type=MESH
@@ -345,15 +342,6 @@
     mix_hi[...] = high
     mix_lo[...] = (mixing - high.astype(f32)).astype(bf16)
 
-    for copy in own_s:
-        copy.wait()
-    shared = dot(nx[0], w_sh[0:1024, :])
-    for q in range(1, 4):
-        shared = shared + dot(nx[q], w_sh[1024 * q : 1024 * q + 1024, :])
-    g, u = shared[:, 0:128], shared[:, 128:256]
-    sh[...] = (g / (1.0 + jnp.exp(-g)) * u).astype(bf16)
-    swaps[0].start()
-
     def scatter(part, recv, send_sem, recv_sem, ch):
         return [
             remote(
@@ -473,6 +461,15 @@
         gts[0, :, cols] = (gate[:, cols] * states).astype(bf16)
 
     swaps[6].start()
+
+    for copy in own_s:
+        copy.wait()
+    shared = dot(nx[0], w_sh[0:1024, :])
+    for q in range(1, 4):
+        shared = shared + dot(nx[q], w_sh[1024 * q : 1024 * q + 1024, :])
+    g, u = shared[:, 0:128], shared[:, 128:256]
+    sh[...] = (g / (1.0 + jnp.exp(-g)) * u).astype(bf16)
+    swaps[0].start()
 
     own_o.wait()
     swaps[1].wait_recv()

time: 79.4 us -> 78.7 us (level)
  Pallas kernels: 78.6 us -> 77.8 us
where the time goes in v6:
time: 78.7 us; the launch traced here: 78.5 us
  Pallas kernels  77.8 us (99%)
    pallas_call x1, Pallas kernels, body(): pl.pallas_call(whole_kernel, out_shape=[jax.ShapeDtypeStruct((32, 4096),...  76 us
    pallas_call x1, Pallas kernels, body(): pl.pallas_call(hand_out, out_shape=[jax.ShapeDtypeStruct((32, 4096), bf16...  1.84 us

profile of v6, /device:TPU:1, one launch (start us, length us, event | category | flops | bytes accessed | tf_op | source)
XLA Modules:
  0.0 78.5 jit_solution(4682057702874252618)
XLA Ops:
  0.6 76.0 %shard_map.212 = (bf16[32,4096]{1,0:T(8,128)(2,1)}, bf16[32,4096]{1,0:T(8,128)(2,1)}) custom-call(bf16[256,4096]{1,0:T(8,128)(2,1)} %m_rows.1, bf16[4096,512]{1,0:T(8,128)(2,1)} %g_proj.1, bf16[4096,512]{1,0:T(8,128)(2,1)} %i_proj.1, bf16[2,256,256]{2,1,0:T(8,128)(2,1)} %i_gates.1, bf16[2,256,256]{2,1,0:T(8,128)(2,1)} %d_gates.1, bf16[512,4096]{1,0:T(8,128)(2,1)} %op.1, ...), custom_call_target="tpu_custom_call" | custom-call | tf_op jit(solution)/shard_map/pallas_call | solution.py:578
  76.7 1.8 %shard_map.213 = (bf16[32,4096]{1,0:T(8,128)(2,1)}, bf16[32,4096]{1,0:T(8,128)(2,1)}) custom-call(bf16[32,4096]{1,0:T(8,128)(2,1)} %get-tuple-element.4.a, bf16[32,4096]{1,0:T(8,128)(2,1)} %get-tuple-element.5.b), custom_call_target="tpu_custom_call" | custom-call | tf_op jit(solution)/shard_map/pallas_call | solution.py:653
